TPU v7x, 768 devices: a whole 4x8x12 slice. The times are simulated.
768 devices in a mesh: ep: 48 (over z, x), tp: 16 (over y, core).
Axes of the slice: x: 4, y: 8, z: 12, core: 2. Of those that a mesh axis runs over, the one named last changes fastest.
Arguments:
- tokens: bfloat16 [122880, 2048], P(('ep', 'tp')), may hold values from -6 to 6
- expert_ids: int32 [122880, 2], P(('ep', 'tp')), may hold values from 0 to 47, all different within a row; in each aligned block of 160 rows (0 to 159, 160 to 319, ...) at most 10 rows name the same one
- group_weight: float32 [122880], P(('ep', 'tp')), may hold values from 0.3 to 1
- expert_share: float32 [122880, 2], P(('ep', 'tp')), may hold values from 0.05 to 1
- gate_w: bfloat16 [48, 512, 2048], P('ep', 'tp'), may hold values from -0.125 to 0.125
- up_w: bfloat16 [48, 512, 2048], P('ep', 'tp'), may hold values from -0.125 to 0.125
- down_w: bfloat16 [48, 512, 2048], P('ep', 'tp'), may hold values from -0.25 to 0.25
- out_gain: float32 [2048], replicated, may hold values from 0.1 to 1.9
- out_shift: float32 [2048], replicated, may hold values from -3 to 3
Outputs:
- layer_out: bfloat16 [122880, 2048], P(('ep', 'tp'))
Inputs may be any that keep to these rules, and one draw needn't show every extreme that they name: `expert_ids`: the 2 ids of a token differ. Among the rows of one device no id is named more than 10 times, and in some device's rows some id is named exactly 10 times.
All inputs are finite; a program needn't handle non-finite values.
Results may differ from a plain program's by a relative error of at most 0.0021.
Values may be sent and summed in bfloat16 or wider, within the bound.
No kernel may reach another device: no remote copies, remote signals or barrier semaphores. Data moves between devices by JAX's collectives and lax.ppermute only.
A program may use at most 32 MiB of HBM per device.

v0:
```python
import jax
import jax.numpy as jnp
from jax import lax
from jax.sharding import PartitionSpec as P

TOP = 2


residual_scale = 2.0**0.5
norm_eps = 1e-05


def in_one_piece(arrays, axis, dim, along):
    ends, at = ([], 0)
    for a in arrays[:-1]:
        at += a.shape[along]
        ends.append(at)
    both = jnp.concatenate(arrays, axis=along)
    return tuple(jnp.split(lax.all_gather(both, axis, axis=dim, tiled=True), ends, axis=along))


def layer_norm(values, gain, shift):
    center = values - jnp.mean(values, axis=-1, keepdims=True)
    variance = jnp.mean(center * center, axis=-1, keepdims=True)
    return (center * lax.rsqrt(variance + norm_eps) * gain + shift).astype(jnp.bfloat16)


def body(tokens, expert_ids, group_weight, expert_share, gate_w, up_w, down_w, out_gain, out_shift):
    tok_count, model_width = tokens.shape
    ep_size = lax.axis_size("ep")
    local_count = gate_w.shape[0]
    experts_all = ep_size * local_count
    capacity = 3 * tok_count * TOP // (2 * experts_all)
    gathered = in_one_piece((gate_w, up_w, down_w), "tp", 1, 0)
    flat_ids = expert_ids.reshape(-1)
    onehot = (flat_ids[:, None] == jnp.arange(experts_all, dtype=jnp.int32)[None, :]).astype(
        jnp.int32
    )
    earlier = jnp.cumsum(onehot, axis=0) - onehot
    slot_index = jnp.sum(earlier * onehot, axis=1)
    dest_index = flat_ids * capacity + slot_index
    copies = jnp.repeat(tokens, TOP, axis=0)
    send_buf = (
        jnp.zeros((experts_all * capacity, model_width), tokens.dtype).at[dest_index].set(copies)
    )
    send_buf = send_buf.reshape(ep_size, local_count * capacity, model_width)
    received = lax.all_to_all(send_buf, "ep", split_axis=0, concat_axis=0, tiled=True)
    expert_rows = received.reshape(ep_size, local_count, capacity, model_width)
    expert_rows = expert_rows.transpose(1, 0, 2, 3).reshape(
        local_count, ep_size * capacity, model_width
    )
    gate_piece, up_piece, down_piece = gathered
    gate_act = jnp.einsum(
        "lrd,lfd->lrf", expert_rows, gate_piece, preferred_element_type=jnp.float32
    )
    up_act = jnp.einsum("lrd,lfd->lrf", expert_rows, up_piece, preferred_element_type=jnp.float32)
    hidden = (jax.nn.silu(gate_act) * up_act).astype(jnp.bfloat16)
    expert_out = jnp.einsum("lrf,lfd->lrd", hidden, down_piece, preferred_element_type=jnp.float32)
    results = expert_out.astype(jnp.bfloat16).reshape(local_count, ep_size, capacity, model_width)
    results = results.transpose(1, 0, 2, 3).reshape(ep_size, local_count * capacity, model_width)
    returned = lax.all_to_all(results, "ep", split_axis=0, concat_axis=0, tiled=True)
    returned = returned.reshape(experts_all * capacity, model_width)
    picked = returned[dest_index].reshape(tok_count, TOP, model_width)
    share_norm = expert_share / jnp.sum(expert_share, axis=1, keepdims=True)
    route_weight = group_weight[:, None] * share_norm
    mixture = jnp.sum(route_weight[:, :, None] * picked.astype(jnp.float32), axis=1)
    residual = residual_scale * tokens.astype(jnp.float32) + mixture
    return layer_norm(residual, out_gain, out_shift)


def solution(mesh):
    placed = (
        P(("ep", "tp"), None),
        P(("ep", "tp"), None),
        P(("ep", "tp")),
        P(("ep", "tp"), None),
        P("ep", "tp", None),
        P("ep", "tp", None),
        P("ep", "tp", None),
        P(),
        P(),
    )
    return jax.shard_map(
        body, mesh=mesh, in_specs=placed, out_specs=P(("ep", "tp"), None), check_vma=False
    )
```

profile of v0, /device:TPU:12, one launch (start us, length us, event | category | flops | bytes accessed | tf_op | source)
XLA Modules:
  0.0 299.1 jit_solution(2733321128681144482)
XLA Ops:
  6.5 1.9 pad_maximum_fusion
  8.4 0.0 all-gather.2.cloned.1.call-update
  8.4 0.8 copy.13
  9.2 0.1 eq.22
  9.4 0.9 reduce-window.6
  10.3 0.2 slice_reduce_fusion
  10.6 0.7 broadcast_multiply_fusion
  11.3 0.1 copy.12
  11.4 0.1 mul.76
  11.5 0.8 broadcast_in_dim.5
  12.3 0.5 reshape.122
  12.9 0.1 bitcast_bitcast_fusion
  13.0 4.0 %scatter_custom_fusion = bf16[480,2048]{1,0:T(8,128)(2,1)} fusion(s32[320]{0:T(512)S(1)} %fusion.13, bf16[320,2048]{1,0:T(8,128)(2,1)S(1)} %reshape.122, bf16[]{:T(256)} %constant.8.clone.1), kind=kCustom, calls=%fused_computation.17 | custom fusion | bytes 1966082 | tf_op jit(solution)/shard_map/scatter | solution.py:44
  17.0 2.6 reshape.102
  19.7 126.7 %all_to_all.10 = bf16[48,10,2048]{2,1,0:T(8,128)(2,1)} all-to-all(bf16[48,10,2048]{2,1,0:T(8,128)(2,1)S(1)} %reshape.102), channel_id=1, replica_groups=mesh['ep'=48,'tp'=16] {'ep'}, dimensions={0} | all-to-all | bytes 3932160 | tf_op jit(solution)/shard_map/all_to_all | solution.py:47
  146.4 2.9 reshape.103
  149.3 0.0 all-gather.2.cloned.1.call-done
  149.4 2.8 fusion.1
  152.2 5.8 %convolution_convert_fusion = bf16[480,2048]{1,0:T(8,128)(2,1)} fusion(bf16[3,512,2048]{2,1,0:T(8,128)(2,1)} %all-gather.2.cloned.1.call-done, bf16[480,2048]{1,0:T(8,128)(2,1)S(1)} %reshape.103, f32[480,512]{1,0:T(8,128)S(1)} %fusion.1), kind=kOutput, calls=%fused_computation.2 | convolution fusion | flops 2015723520 | bytes 9109504 | tf_op jit(solution)/shard_map/lrf,lfd->lrd/dot_general | solution.py:58
  158.0 4.2 %reshape_transpose_reshape.4 = bf16[48,10,2048]{2,1,0:T(8,128)(2,1)} reshape(bf16[480,2048]{1,0:T(8,128)(2,1)} %convolution_convert_fusion) | data formatting | bytes 3932160 | tf_op jit(solution)/shard_map/reshape;transpose;reshape | solution.py:60
  162.2 7.4 %all-to-all-start.1 = ((bf16[48,10,2048]{2,1,0:T(8,128)(2,1)}), bf16[48,10,2048]{2,1,0:T(8,128)(2,1)}, u32[]{:S(2)}, u32[]{:S(2)}) async-start(bf16[48,10,2048]{2,1,0:T(8,128)(2,1)} %reshape_transpose_reshape.4), calls=%async_computation.1 | async-start | bytes 6291456 | tf_op jit(solution)/shard_map/all_to_all | solution.py:61
  169.7 0.1 copy.11
  169.8 107.3 %all-to-all-done.1 = bf16[48,10,2048]{2,1,0:T(8,128)(2,1)} async-done(((bf16[48,10,2048]{2,1,0:T(8,128)(2,1)}), bf16[48,10,2048]{2,1,0:T(8,128)(2,1)}, u32[]{:S(2)}, u32[]{:S(2)}) %all-to-all-start.1) | async-done | bytes 1966112 | tf_op jit(solution)/shard_map/all_to_all | solution.py:61
  277.2 2.9 reshape.107
  280.1 3.0 %gather_fusion = bf16[320,2048]{1,0:T(8,128)(2,1)} fusion(bf16[480,2048]{1,0:T(8,128)(2,1)S(1)} %reshape.107, s32[1024]{0:T(1024)S(1)} %pad_clamp_fusion), kind=kCustom, calls=%fused_computation | custom fusion | bytes 2622720 | tf_op jit(solution)/shard_map/gather | solution.py:63
  283.1 3.1 %reshape.109 = f32[160,2,2048]{2,1,0:T(2,128)S(1)} reshape(bf16[320,2048]{1,0:T(8,128)(2,1)} %gather_fusion) | data formatting | bytes 3932160 | tf_op jit(solution)/shard_map/convert_element_type | solution.py:66
  286.2 4.1 %multiply_reduce_fusion = f32[160,2048]{1,0:T(8,128)S(1)} fusion(f32[160,2,2048]{2,1,0:T(2,128)S(1)} %reshape.109, f32[160,2]{1,0:T(8,128)S(1)} %copy.11), kind=kLoop, calls=%fused_computation.3 | loop fusion | flops 983040 | bytes 3933440 | tf_op jit(solution)/shard_map/reduce_sum | solution.py:66
  290.3 0.3 fusion.10
  290.6 0.4 multiply_reduce_fusion.1
  290.9 0.1 copy-done.2
  291.0 0.0 copy-done.3
  291.0 1.2 add_convert_fusion
  (21 shorter events, 0.2 us)
Async XLA Ops:
  6.5 5.0 %copy-start = (bf16[160,2048]{1,0:T(8,128)(2,1)S(1)}, bf16[160,2048]{1,0:T(8,128)(2,1)}, u32[]{:S(2)}) copy-start(bf16[160,2048]{1,0:T(8,128)(2,1)} %param.9) | copy-start | bytes 1966084
  6.5 142.8 %all-gather.2.cloned.1.call-start = ((), (), s32[]{:S(2)}) async-start(), calls=%async_computation.2 | async-start | bytes 6684672 | tf_op jit(solution)/shard_map/all_gather | solution.py:19
  162.2 7.4 %copy-start.4 = (f32[160,2]{0,1:T(2,128)S(1)}, f32[160,2]{0,1:T(2,128)}, u32[]{:S(2)}) copy-start(f32[160,2]{0,1:T(2,128)} %param.12) | copy-start | bytes 3844
  162.2 7.5 %copy-start.5 = (f32[160]{0:T(256)S(1)}, f32[160]{0:T(256)}, u32[]{:S(2)}) copy-start(f32[160]{0:T(256)} %param.11) | copy-start | bytes 1924
  162.2 115.0 %all-to-all-start.1 = ((bf16[48,10,2048]{2,1,0:T(8,128)(2,1)}), bf16[48,10,2048]{2,1,0:T(8,128)(2,1)}, u32[]{:S(2)}, u32[]{:S(2)}) async-start(bf16[48,10,2048]{2,1,0:T(8,128)(2,1)} %reshape_transpose_reshape.4), calls=%async_computation.1 | async-start | bytes 6291456 | tf_op jit(solution)/shard_map/all_to_all | solution.py:61
  286.2 4.1 %copy-start.1 = (bf16[160,2048]{1,0:T(8,128)(2,1)S(1)}, bf16[160,2048]{1,0:T(8,128)(2,1)}, u32[]{:S(2)}) copy-start(bf16[160,2048]{1,0:T(8,128)(2,1)} %param.9) | copy-start | bytes 1966084
  290.3 0.7 copy-start.2
  290.3 0.7 copy-start.3
Sparse Core Ops, SparseCore 0:
  9.8 57.3 all-gather.1
where the time goes:
time: 300 us; the launch traced here: 299 us
  blocking collectives  127 us (42%)
  waiting for transfers between devices  107 us (36%)
  local copies, waits for them, and re-layouts  25.7 us (9%)
  between operations  13.6 us (5%)
  other arithmetic  9.58 us (3%)
  matrix products  8.64 us (3%)
  starting transfers between devices  7.43 us (2%)
    all_to_all x1, blocking collectives, body(): lax.all_to_all(send_buf, 'ep', split_axis=0, concat_axis=0, tiled=True)  127 us
    all_to_all x1, waiting for transfers between devices, body(): lax.all_to_all(results, 'ep', split_axis=0, concat_axis=0, tiled=True)  107 us
    all_to_all x1, starting transfers between devices, body(): lax.all_to_all(results, 'ep', split_axis=0, concat_axis=0, tiled=True)  7.43 us
  transfers between devices with their start and end apart: 2, of which 1 were waited for; matrix products, arithmetic and copies ran while one was open for 5% of the time, Pallas kernels for 0%

commit v1 on v0

v1 whole, which is shorter than its diff:
```python
import functools

import jax
import jax.numpy as jnp
from jax import lax
from jax.experimental import pallas as pl
from jax.experimental.pallas import tpu as pltpu
from jax.sharding import PartitionSpec as P

TOP = 2
residual_scale = 2.0**0.5
norm_eps = 1e-05
BF16 = jnp.bfloat16
F32 = jnp.float32
HEAD = 8
REST = 2
QUARTERS = 4


def dot(a, b):
    return jnp.dot(a, b, preferred_element_type=F32)


def dot_nt(a, b):
    return lax.dot_general(a, b, (((1,), (1,)), ((), ())), preferred_element_type=F32)


def iota(shape, dim):
    return lax.broadcasted_iota(jnp.int32, shape, dim)


def flag(condition):
    return jnp.where(condition, 1.0, 0.0).astype(BF16)


def pack_kernel(tok_ref, ids_ref, out_ref):
    experts, _, width = out_ref.shape
    count = tok_ref.shape[0]
    expert = iota((experts, count), 0)
    named = (ids_ref[0:1, :] == expert) | (ids_ref[1:2, :] == expert)
    hit = jnp.where(named, 1.0, 0.0)
    before = flag(iota((count, count), 0) < iota((count, count), 1))
    place = hit * (dot(hit.astype(BF16), before) + 1.0)
    slots = experts * HEAD
    spread = flag(iota((slots, experts), 0) // HEAD == iota((slots, experts), 1))
    place = dot(spread, place.astype(BF16))
    row = iota((slots, count), 0)
    in_block = row % HEAD
    head = flag(place == (in_block + 1).astype(F32))
    second = place == (HEAD + 1 + row % REST).astype(F32)
    rest = jnp.zeros((slots, width), F32)
    for q in range(QUARTERS):
        part = tok_ref[:, q * width : (q + 1) * width]
        out_ref[:, q * HEAD : (q + 1) * HEAD, :] = (
            dot(head, part).astype(BF16).reshape(experts, HEAD, width)
        )
        rest += dot(flag(second & (in_block // REST == q)), part)
    out_ref[:, QUARTERS * HEAD :, :] = rest.astype(BF16).reshape(experts, HEAD, width)


def ffn_kernel(gate_steps, recv_ref, gate_ref, up_ref, down_ref, out_ref, rows_ref, hidden_ref, rest_ref):
    step = pl.program_id(0)
    sources, _, width = recv_ref.shape
    heads, rests = sources * HEAD, sources * REST

    def pick(q):
        a = iota((rests, heads), 0)
        return flag(iota((rests, heads), 1) == (a // REST) * HEAD + q * REST + a % REST)

    def spread(q):
        a = iota((heads, rests), 1)
        return flag(iota((heads, rests), 0) == (a // REST) * HEAD + q * REST + a % REST)

    @pl.when(step == 0)
    def _():
        rest = recv_ref[:, QUARTERS * HEAD :, :].reshape(heads, width)
        for q in range(QUARTERS):
            cols = slice(q * width, (q + 1) * width)
            rows_ref[0:heads, cols] = recv_ref[:, q * HEAD : (q + 1) * HEAD, :].reshape(heads, width)
            rows_ref[heads:, cols] = dot(pick(q), rest).astype(BF16)

    for i in range(gate_steps):

        @pl.when(step == i)
        def _():
            rows = rows_ref[...]
            gate = dot_nt(rows, gate_ref[...])
            up = dot_nt(rows, up_ref[...])
            size = gate_ref.shape[0]
            hidden_ref[:, i * size : (i + 1) * size] = (
                gate / (1.0 + jnp.exp(-gate)) * up
            ).astype(BF16)

    for q in range(QUARTERS):

        @pl.when(step == gate_steps + q)
        def _():
            result = dot(hidden_ref[...], down_ref[...]).astype(BF16)
            out_ref[:, q * HEAD : (q + 1) * HEAD, :] = result[0:heads].reshape(sources, HEAD, width)
            part = dot(spread(q), result[heads:])
            if q == 0:
                rest_ref[...] = part
            elif q < QUARTERS - 1:
                rest_ref[...] += part
            else:
                out_ref[:, QUARTERS * HEAD :, :] = (
                    (rest_ref[...] + part).astype(BF16).reshape(sources, HEAD, width)
                )


def mix_kernel(back_ref, tok_ref, ids_ref, weight_ref, gain_ref, shift_ref, out_ref, sum_ref):
    experts, _, width = back_ref.shape
    count, model_width = tok_ref.shape
    expert = iota((count, experts), 1)
    first, last = ids_ref[:, 0:1] == expert, ids_ref[:, 1:2] == expert
    hit = jnp.where(first | last, 1.0, 0.0)
    before = flag(iota((count, count), 1) < iota((count, count), 0))
    place = hit * (dot(before, hit.astype(BF16)) + 1.0)
    weight = jnp.where(first, weight_ref[:, 0:1], 0.0) + jnp.where(last, weight_ref[:, 1:2], 0.0)
    high = weight.astype(BF16)
    low = (weight - high.astype(F32)).astype(BF16)
    slots = experts * HEAD
    spread = flag(iota((experts, slots), 1) // HEAD == iota((experts, slots), 0))
    place = dot(place.astype(BF16), spread)
    high, low = dot(high, spread), dot(low, spread)
    column = iota((count, slots), 1)
    in_block = column % HEAD

    def chosen(condition):
        return (
            jnp.where(condition, high, 0.0).astype(BF16),
            jnp.where(condition, low, 0.0).astype(BF16),
        )

    head_high, head_low = chosen(place == (in_block + 1).astype(F32))
    second = place == (HEAD + 1 + column % REST).astype(F32)
    rest = back_ref[:, QUARTERS * HEAD :, :].reshape(slots, width)
    total = jnp.zeros((count, 1), F32)
    for q in range(QUARTERS):
        cols = slice(q * width, (q + 1) * width)
        head = back_ref[:, q * HEAD : (q + 1) * HEAD, :].reshape(slots, width)
        rest_high, rest_low = chosen(second & (in_block // REST == q))
        mixture = dot(head_high, head) + dot(rest_high, rest)
        mixture += dot(head_low, head) + dot(rest_low, rest)
        residual = residual_scale * tok_ref[:, cols].astype(F32) + mixture
        sum_ref[:, cols] = residual
        total += jnp.sum(residual, axis=-1, keepdims=True)
    center = sum_ref[...] - total / model_width
    variance = jnp.mean(center * center, axis=-1, keepdims=True)
    out_ref[...] = (center * lax.rsqrt(variance + norm_eps) * gain_ref[...] + shift_ref[...]).astype(BF16)


def body(tokens, expert_ids, group_weight, expert_share, gate_w, up_w, down_w, out_gain, out_shift):
    tok_count, model_width = tokens.shape
    ep_size = lax.axis_size("ep")
    width = model_width // QUARTERS
    block = (HEAD + REST) * QUARTERS
    hidden = gate_w.shape[1] * lax.axis_size("tp")
    gate, up, down = (
        lax.all_gather(w[0], "tp", axis=0, tiled=True) for w in (gate_w, up_w, down_w)
    )
    buffer = jax.ShapeDtypeStruct((ep_size, block, width), BF16)
    send = pl.pallas_call(
        pack_kernel,
        out_shape=buffer,
        name="pack",
    )(tokens, expert_ids.T)
    received = lax.all_to_all(send, "ep", split_axis=0, concat_axis=0, tiled=True)
    gate_steps = 2
    rows = ep_size * (HEAD + REST)
    results = pl.pallas_call(
        functools.partial(ffn_kernel, gate_steps),
        out_shape=buffer,
        grid=(gate_steps + QUARTERS,),
        in_specs=[
            pl.BlockSpec((ep_size, block, width), lambda i: (0, 0, 0)),
            pl.BlockSpec((hidden // gate_steps, model_width), lambda i: (jnp.minimum(i, gate_steps - 1), 0)),
            pl.BlockSpec((hidden // gate_steps, model_width), lambda i: (jnp.minimum(i, gate_steps - 1), 0)),
            pl.BlockSpec((hidden, width), lambda i: (0, jnp.maximum(i - gate_steps, 0))),
        ],
        out_specs=pl.BlockSpec((ep_size, block, width), lambda i: (0, 0, 0)),
        scratch_shapes=[
            pltpu.VMEM((rows, model_width), BF16),
            pltpu.VMEM((rows, hidden), BF16),
            pltpu.VMEM((ep_size * HEAD, width), F32),
        ],
        name="ffn",
    )(received, gate, up, down)
    back = lax.all_to_all(results, "ep", split_axis=0, concat_axis=0, tiled=True)
    share_norm = expert_share / jnp.sum(expert_share, axis=1, keepdims=True)
    route_weight = group_weight[:, None] * share_norm
    return pl.pallas_call(
        mix_kernel,
        out_shape=jax.ShapeDtypeStruct((tok_count, model_width), BF16),
        scratch_shapes=[pltpu.VMEM((tok_count, model_width), F32)],
        name="mix",
    )(back, tokens, expert_ids, route_weight, out_gain[None], out_shift[None])


def solution(mesh):
    placed = (
        P(("ep", "tp"), None),
        P(("ep", "tp"), None),
        P(("ep", "tp")),
        P(("ep", "tp"), None),
        P("ep", "tp", None),
        P("ep", "tp", None),
        P("ep", "tp", None),
        P(),
        P(),
    )
    return jax.shard_map(
        body, mesh=mesh, in_specs=placed, out_specs=P(("ep", "tp"), None), check_vma=False
    )
```

time: 300 us -> 263 us (0.88)
  the two profiles are of different devices: /device:TPU:12 before, /device:TPU:1 now
where the time goes in v1:
time: 263 us; the launch traced here: 262 us
  waiting for transfers between devices  193 us (73%)
  starting transfers between devices  32.1 us (12%)
  Pallas kernels  19.2 us (7%)
  between operations  13.2 us (5%)
  local copies, waits for them, and re-layouts  3.52 us (1%)
    all_gather x3, waiting for transfers between devices, body(): lax.all_gather(w[0], 'tp', axis=0, tiled=True)  123 us
    all_to_all x1, waiting for transfers between devices, body(): lax.all_to_all(results, 'ep', split_axis=0, concat_axis=0, tiled=True)  68 us
    all_to_all x1, starting transfers between devices, body(): lax.all_to_all(send, 'ep', split_axis=0, concat_axis=0, tiled=True)  18.8 us
    all_to_all x1, starting transfers between devices, body(): lax.all_to_all(results, 'ep', split_axis=0, concat_axis=0, tiled=True)  13.1 us
    pallas_call x1, Pallas kernels, body(): pl.pallas_call(functools.partial(ffn_kernel, gate_steps), out_shape=buffe...  10.6 us
  transfers between devices with their start and end apart: 5, of which 4 were waited for; matrix products, arithmetic and copies ran while one was open for 1% of the time, Pallas kernels for 1%

profile of v1, /device:TPU:1, one launch (start us, length us, event | category | flops | bytes accessed | tf_op | source)
XLA Modules:
  0.0 261.5 jit_solution(1108522133164790364)
XLA Ops:
  6.5 0.0 all-gather.7.cloned.1.call-start
  6.5 0.7 all-gather.7.cloned.1.call-update
  7.3 0.0 all-gather.9.cloned.1.call-start
  7.3 0.7 all-gather.9.cloned.1.call-update
  8.0 3.6 %pack.1 = bf16[48,40,512]{2,1,0:T(8,128)(2,1)} custom-call(bf16[160,2048]{1,0:T(8,128)(2,1)} %tok_ref.3, s32[2,160]{1,0:T(2,128)} %bitcast.11), custom_call_target="tpu_custom_call" | custom-call | tf_op jit(solution)/shard_map/pack/pallas_call | solution.py:163
  11.7 18.8 %all-to-all-start = ((bf16[48,40,512]{2,1,0:T(8,128)(2,1)}), bf16[48,40,512]{2,1,0:T(8,128)(2,1)S(1)}, u32[]{:S(2)}, u32[]{:S(2)}) async-start(bf16[48,40,512]{2,1,0:T(8,128)(2,1)} %pack.1), calls=%async_computation | async-start | bytes 3932160 | tf_op jit(solution)/shard_map/all_to_all | solution.py:168
  30.5 0.0 all-gather.11.cloned.1.call-start
  30.5 0.7 all-gather.11.cloned.1.call-update
  31.2 30.9 %all-gather.7.cloned.1.call-done = bf16[1,512,2048]{2,1,0:T(8,128)(2,1)} async-done(((bf16[1,32,2048]{2,1,0:T(8,128)(2,1)}), bf16[1,512,2048]{2,1,0:T(8,128)(2,1)}) %all-gather.7.cloned.1.call-update) | async-done | bytes 2097168 | tf_op jit(solution)/shard_map/all_gather | solution.py:160
  62.2 45.9 %all-gather.9.cloned.1.call-done = bf16[1,512,2048]{2,1,0:T(8,128)(2,1)} async-done(((bf16[1,32,2048]{2,1,0:T(8,128)(2,1)}), bf16[1,512,2048]{2,1,0:T(8,128)(2,1)}) %all-gather.9.cloned.1.call-update) | async-done | bytes 2097168 | tf_op jit(solution)/shard_map/all_gather | solution.py:160
  108.1 46.0 %all-gather.11.cloned.1.call-done = bf16[1,512,2048]{2,1,0:T(8,128)(2,1)} async-done(((bf16[1,32,2048]{2,1,0:T(8,128)(2,1)}), bf16[1,512,2048]{2,1,0:T(8,128)(2,1)}) %all-gather.11.cloned.1.call-update) | async-done | bytes 2097168 | tf_op jit(solution)/shard_map/all_gather | solution.py:160
  154.1 0.0 all-to-all-done.recv_ref
  154.1 0.0 copy-start
  154.1 1.3 copy-done
  155.4 10.6 %ffn.1 = bf16[48,40,512]{2,1,0:T(8,128)(2,1)} custom-call(bf16[48,40,512]{2,1,0:T(8,128)(2,1)} %copy-done, bf16[512,2048]{1,0:T(8,128)(2,1)} %bitcast.6, bf16[512,2048]{1,0:T(8,128)(2,1)} %bitcast.7, bf16[512,2048]{1,0:T(8,128)(2,1)} %bitcast.8), custom_call_target="tpu_custom_call" | custom-call | tf_op jit(solution)/shard_map/ffn/pallas_call | solution.py:171
  166.0 0.0 copy-start.3
  166.0 0.0 copy-start.2
  166.0 0.0 copy-start.4
  166.0 13.1 %all-to-all-start.1 = ((bf16[48,40,512]{2,1,0:T(8,128)(2,1)}), bf16[48,40,512]{2,1,0:T(8,128)(2,1)S(1)}, u32[]{:S(2)}, u32[]{:S(2)}) async-start(bf16[48,40,512]{2,1,0:T(8,128)(2,1)} %ffn.1), calls=%async_computation.1 | async-start | bytes 3932160 | tf_op jit(solution)/shard_map/all_to_all | solution.py:189
  179.2 0.0 copy-done.3
  179.2 0.7 copy.15.ids_ref
  179.9 0.0 copy-done.2
  180.0 0.1 copy.14
  180.1 0.0 copy-done.4
  180.1 0.7 broadcast_multiply_fusion.weight_ref
  180.8 68.0 %all-to-all-done.1.back_ref = bf16[48,40,512]{2,1,0:T(8,128)(2,1)S(1)} async-done(((bf16[48,40,512]{2,1,0:T(8,128)(2,1)}), bf16[48,40,512]{2,1,0:T(8,128)(2,1)S(1)}, u32[]{:S(2)}, u32[]{:S(2)}) %all-to-all-start.1) | async-done | bytes 1966112 | tf_op jit(solution)/shard_map/all_to_all | solution.py:189
  248.8 0.0 copy-start.1
  248.8 1.3 copy-done.1
  250.1 4.9 %mix.1 = bf16[160,2048]{1,0:T(8,128)(2,1)} custom-call(bf16[48,40,512]{2,1,0:T(8,128)(2,1)} %copy-done.1, bf16[160,2048]{1,0:T(8,128)(2,1)} %tok_ref.3, s32[160,2]{1,0:T(8,128)} %copy.15.ids_ref, f32[160,2]{1,0:T(8,128)} %broadcast_multiply_fusion.weight_ref, f32[1,2048]{1,0:T(1,128)} %bitcast.9, f32[1,2048]{1,0:T(1,128)} %bitcast.10), custom_call_target="tpu_custom_call" | custom-call | tf_op jit(solution)/shard_map/mix/pallas_call | solution.py:192
  (2 shorter events, 0.0 us)
Async XLA Ops:
  6.5 55.6 %all-gather.7.cloned.1.call-start = ((), (), s32[]{:S(2)}) async-start(), calls=%async_computation.2 | async-start | bytes 2228224 | tf_op jit(solution)/shard_map/all_gather | solution.py:160
  7.3 100.8 %all-gather.9.cloned.1.call-start = ((), (), s32[]{:S(2)}) async-start(), calls=%async_computation.3 | async-start | bytes 2228224 | tf_op jit(solution)/shard_map/all_gather | solution.py:160
  11.7 142.4 %all-to-all-start = ((bf16[48,40,512]{2,1,0:T(8,128)(2,1)}), bf16[48,40,512]{2,1,0:T(8,128)(2,1)S(1)}, u32[]{:S(2)}, u32[]{:S(2)}) async-start(bf16[48,40,512]{2,1,0:T(8,128)(2,1)} %pack.1), calls=%async_computation | async-start | bytes 3932160 | tf_op jit(solution)/shard_map/all_to_all | solution.py:168
  30.5 123.6 %all-gather.11.cloned.1.call-start = ((), (), s32[]{:S(2)}) async-start(), calls=%async_computation.4 | async-start | bytes 2228224 | tf_op jit(solution)/shard_map/all_gather | solution.py:160
  154.1 1.3 copy-start
  166.0 13.2 %copy-start.3 = (s32[160,2]{0,1:T(2,128)S(1)}, s32[160,2]{0,1:T(2,128)}, u32[]{:S(2)}) copy-start(s32[160,2]{0,1:T(2,128)} %param.10) | copy-start | bytes 3844
  166.0 13.9 %copy-start.2 = (f32[160,2]{0,1:T(2,128)S(1)}, f32[160,2]{0,1:T(2,128)}, u32[]{:S(2)}) copy-start(f32[160,2]{0,1:T(2,128)} %param.12) | copy-start | bytes 3844
  166.0 14.1 %copy-start.4 = (f32[160]{0:T(256)S(1)}, f32[160]{0:T(256)}, u32[]{:S(2)}) copy-start(f32[160]{0:T(256)} %param.11) | copy-start | bytes 1924
  166.0 82.8 %all-to-all-start.1 = ((bf16[48,40,512]{2,1,0:T(8,128)(2,1)}), bf16[48,40,512]{2,1,0:T(8,128)(2,1)S(1)}, u32[]{:S(2)}, u32[]{:S(2)}) async-start(bf16[48,40,512]{2,1,0:T(8,128)(2,1)} %ffn.1), calls=%async_computation.1 | async-start | bytes 3932160 | tf_op jit(solution)/shard_map/all_to_all | solution.py:189
  248.8 1.3 copy-start.1
Sparse Core Ops, SparseCore 0:
  9.7 52.3 all-gather.6
  64.6 43.4 all-gather.8
  110.5 43.5 all-gather.10

commit v2 on v1

--- a/solution.py
+++ b/solution.py
@@ -15,6 +15,8 @@
 HEAD = 8
 REST = 2
 QUARTERS = 4
+SLICE = 32
+ROOM = 52 * 2**20
 
 
 def dot(a, b):
@@ -33,7 +35,14 @@
     return jnp.where(condition, 1.0, 0.0).astype(BF16)
 
 
-def pack_kernel(tok_ref, ids_ref, out_ref):
+def send_out(staged_ref, out_ref, sems, j):
+    rows = pl.ds(j * HEAD, HEAD)
+    copy = pltpu.make_async_copy(staged_ref.at[j], out_ref.at[:, rows, :], sems.at[j])
+    copy.start()
+    return copy
+
+
+def pack_kernel(tok_ref, ids_ref, out_ref, staged_ref, sems):
     experts, _, width = out_ref.shape
     count = tok_ref.shape[0]
     expert = iota((experts, count), 0)
@@ -49,19 +58,44 @@
     head = flag(place == (in_block + 1).astype(F32))
     second = place == (HEAD + 1 + row % REST).astype(F32)
     rest = jnp.zeros((slots, width), F32)
+    copies = []
     for q in range(QUARTERS):
         part = tok_ref[:, q * width : (q + 1) * width]
-        out_ref[:, q * HEAD : (q + 1) * HEAD, :] = (
-            dot(head, part).astype(BF16).reshape(experts, HEAD, width)
-        )
+        staged_ref[q] = dot(head, part).astype(BF16).reshape(experts, HEAD, width)
+        copies.append(send_out(staged_ref, out_ref, sems, q))
         rest += dot(flag(second & (in_block // REST == q)), part)
-    out_ref[:, QUARTERS * HEAD :, :] = rest.astype(BF16).reshape(experts, HEAD, width)
-
-
-def ffn_kernel(gate_steps, recv_ref, gate_ref, up_ref, down_ref, out_ref, rows_ref, hidden_ref, rest_ref):
-    step = pl.program_id(0)
+    staged_ref[QUARTERS] = rest.astype(BF16).reshape(experts, HEAD, width)
+    copies.append(send_out(staged_ref, out_ref, sems, QUARTERS))
+    for copy in copies:
+        copy.wait()
+
+
+def ffn_kernel(chunks, recv_ref, *refs):
+    pieces, (out_ref, gate_ref, up_ref, down_ref, rows_ref, hidden_ref, staged_ref, sems, out_sems) = (
+        refs[:-9],
+        refs[-9:],
+    )
     sources, _, width = recv_ref.shape
     heads, rests = sources * HEAD, sources * REST
+    hidden = gate_ref.shape[0]
+
+    waits = []
+    for piece in pieces:
+        for base in range(0, piece.shape[0], 3 * SLICE):
+            at = len(waits)
+            copies = [
+                pltpu.make_async_copy(
+                    piece.at[pl.ds(base + j * SLICE, SLICE), :],
+                    weight.at[pl.ds(at * SLICE, SLICE), :],
+                    sems.at[at, j],
+                )
+                for j, weight in enumerate((gate_ref, up_ref, down_ref))
+            ]
+            copies[0].start()
+            copies[1].start()
+            waits.append(copies)
+    for copies in waits:
+        copies[2].start()
 
     def pick(q):
         a = iota((rests, heads), 0)
@@ -71,41 +105,35 @@
         a = iota((heads, rests), 1)
         return flag(iota((heads, rests), 0) == (a // REST) * HEAD + q * REST + a % REST)
 
-    @pl.when(step == 0)
-    def _():
-        rest = recv_ref[:, QUARTERS * HEAD :, :].reshape(heads, width)
-        for q in range(QUARTERS):
-            cols = slice(q * width, (q + 1) * width)
-            rows_ref[0:heads, cols] = recv_ref[:, q * HEAD : (q + 1) * HEAD, :].reshape(heads, width)
-            rows_ref[heads:, cols] = dot(pick(q), rest).astype(BF16)
-
-    for i in range(gate_steps):
-
-        @pl.when(step == i)
-        def _():
-            rows = rows_ref[...]
-            gate = dot_nt(rows, gate_ref[...])
-            up = dot_nt(rows, up_ref[...])
-            size = gate_ref.shape[0]
-            hidden_ref[:, i * size : (i + 1) * size] = (
-                gate / (1.0 + jnp.exp(-gate)) * up
-            ).astype(BF16)
-
-    for q in range(QUARTERS):
-
-        @pl.when(step == gate_steps + q)
-        def _():
-            result = dot(hidden_ref[...], down_ref[...]).astype(BF16)
-            out_ref[:, q * HEAD : (q + 1) * HEAD, :] = result[0:heads].reshape(sources, HEAD, width)
-            part = dot(spread(q), result[heads:])
-            if q == 0:
-                rest_ref[...] = part
-            elif q < QUARTERS - 1:
-                rest_ref[...] += part
-            else:
-                out_ref[:, QUARTERS * HEAD :, :] = (
-                    (rest_ref[...] + part).astype(BF16).reshape(sources, HEAD, width)
-                )
+    rest = recv_ref[:, QUARTERS * HEAD :, :].reshape(heads, width)
+    for q in range(QUARTERS):
+        cols = slice(q * width, (q + 1) * width)
+        rows_ref[0:heads, cols] = recv_ref[:, q * HEAD : (q + 1) * HEAD, :].reshape(heads, width)
+        rows_ref[heads:, cols] = dot(pick(q), rest).astype(BF16)
+
+    size = hidden // chunks
+    for i in range(chunks):
+        for copies in waits[i * size // SLICE : (i + 1) * size // SLICE]:
+            copies[0].wait()
+            copies[1].wait()
+        part = slice(i * size, (i + 1) * size)
+        gate = dot_nt(rows_ref[...], gate_ref[part, :])
+        up = dot_nt(rows_ref[...], up_ref[part, :])
+        hidden_ref[:, part] = (gate / (1.0 + jnp.exp(-gate)) * up).astype(BF16)
+
+    for copies in waits:
+        copies[2].wait()
+    rest = jnp.zeros((heads, width), F32)
+    sent = []
+    for q in range(QUARTERS):
+        result = dot(hidden_ref[...], down_ref[:, q * width : (q + 1) * width]).astype(BF16)
+        staged_ref[q] = result[0:heads].reshape(sources, HEAD, width)
+        sent.append(send_out(staged_ref, out_ref, out_sems, q))
+        rest += dot(spread(q), result[heads:])
+    staged_ref[QUARTERS] = rest.astype(BF16).reshape(sources, HEAD, width)
+    sent.append(send_out(staged_ref, out_ref, out_sems, QUARTERS))
+    for copy in sent:
+        copy.wait()
 
 
 def mix_kernel(back_ref, tok_ref, ids_ref, weight_ref, gain_ref, shift_ref, out_ref, sum_ref):
@@ -150,49 +178,71 @@
     out_ref[...] = (center * lax.rsqrt(variance + norm_eps) * gain_ref[...] + shift_ref[...]).astype(BF16)
 
 
+def gather_slices(own):
+    size = lax.axis_size("tp")
+    partner = [(i, i ^ 1) for i in range(size)]
+    onward = [(i, (i + 2 - 4 * (i % 2)) % size) for i in range(size)]
+    other = lax.ppermute(own, "tp", partner)
+    pieces = [own, other]
+    moving = jnp.concatenate([own, other], axis=0)
+    steps = size // 4
+    for step in range(steps):
+        if step == steps - 1:
+            moving = moving[: own.shape[0]]
+        moving = lax.ppermute(moving, "tp", onward)
+        pieces += [moving, lax.ppermute(moving, "tp", partner)]
+    return pieces
+
+
 def body(tokens, expert_ids, group_weight, expert_share, gate_w, up_w, down_w, out_gain, out_shift):
     tok_count, model_width = tokens.shape
     ep_size = lax.axis_size("ep")
     width = model_width // QUARTERS
     block = (HEAD + REST) * QUARTERS
     hidden = gate_w.shape[1] * lax.axis_size("tp")
-    gate, up, down = (
-        lax.all_gather(w[0], "tp", axis=0, tiled=True) for w in (gate_w, up_w, down_w)
-    )
     buffer = jax.ShapeDtypeStruct((ep_size, block, width), BF16)
+    vmem = pl.BlockSpec(memory_space=pltpu.VMEM)
+    hbm = pl.BlockSpec(memory_space=pltpu.HBM)
+    staged = pltpu.VMEM((QUARTERS + 1, ep_size, HEAD, width), BF16)
+    staged_sems = pltpu.SemaphoreType.DMA((QUARTERS + 1,))
+    limit = pltpu.CompilerParams(vmem_limit_bytes=32 * 2**20)
     send = pl.pallas_call(
         pack_kernel,
         out_shape=buffer,
+        out_specs=hbm,
+        scratch_shapes=[staged, staged_sems],
         name="pack",
     )(tokens, expert_ids.T)
     received = lax.all_to_all(send, "ep", split_axis=0, concat_axis=0, tiled=True)
-    gate_steps = 2
+    own = jnp.concatenate([gate_w[0], up_w[0], down_w[0]], axis=0)
+    pieces = gather_slices(own)
     rows = ep_size * (HEAD + REST)
     results = pl.pallas_call(
-        functools.partial(ffn_kernel, gate_steps),
+        functools.partial(ffn_kernel, 2),
         out_shape=buffer,
-        grid=(gate_steps + QUARTERS,),
-        in_specs=[
-            pl.BlockSpec((ep_size, block, width), lambda i: (0, 0, 0)),
-            pl.BlockSpec((hidden // gate_steps, model_width), lambda i: (jnp.minimum(i, gate_steps - 1), 0)),
-            pl.BlockSpec((hidden // gate_steps, model_width), lambda i: (jnp.minimum(i, gate_steps - 1), 0)),
-            pl.BlockSpec((hidden, width), lambda i: (0, jnp.maximum(i - gate_steps, 0))),
-        ],
-        out_specs=pl.BlockSpec((ep_size, block, width), lambda i: (0, 0, 0)),
-        scratch_shapes=[
+        in_specs=[vmem] + [hbm] * len(pieces),
+        out_specs=hbm,
+        scratch_shapes=[pltpu.VMEM((hidden, model_width), BF16)] * 3
+        + [
             pltpu.VMEM((rows, model_width), BF16),
             pltpu.VMEM((rows, hidden), BF16),
-            pltpu.VMEM((ep_size * HEAD, width), F32),
+            staged,
+            pltpu.SemaphoreType.DMA((hidden // SLICE, 3)),
+            staged_sems,
         ],
+        compiler_params=pltpu.CompilerParams(vmem_limit_bytes=ROOM),
         name="ffn",
-    )(received, gate, up, down)
+    )(received, *pieces)
     back = lax.all_to_all(results, "ep", split_axis=0, concat_axis=0, tiled=True)
     share_norm = expert_share / jnp.sum(expert_share, axis=1, keepdims=True)
     route_weight = group_weight[:, None] * share_norm
     return pl.pallas_call(
         mix_kernel,
         out_shape=jax.ShapeDtypeStruct((tok_count, model_width), BF16),
+        in_specs=[vmem] * 6,
+        out_specs=vmem,
         scratch_shapes=[pltpu.VMEM((tok_count, model_width), F32)],
+        compiler_params=limit,
         name="mix",
     )(back, tokens, expert_ids, route_weight, out_gain[None], out_shift[None])
 

time: 263 us -> 185 us (0.70)
  waiting for transfers between devices: 193 us -> 96.6 us
  starting transfers between devices: 32.1 us -> 64.9 us
  between operations: 13.2 us -> 0.35 us
  Pallas kernels: 19.2 us -> 16.2 us
    all_gather x3 -> x0, waiting for transfers between devices: 123 us -> none  [body(): lax.all_gather(w[0], 'tp', axis=0, tiled=True)]
    ppermute x0 -> x9, starting transfers between devices: none -> 36.3 us  [the longest x4 21 us: gather_slices(): moving = lax.ppermute(moving, 'tp', onward)]
    ppermute x0 -> x9, waiting for transfers between devices: none -> 26.5 us  [the longest x4 25.2 us: gather_slices(): moving = lax.ppermute(moving, 'tp', onward)]
    all_to_all x1, starting transfers between devices: 13.1 us -> 9.6 us  [body(): lax.all_to_all(results, 'ep', split_axis=0, concat_axis=0, tiled=True)]
    all_to_all x1, waiting for transfers between devices: 0.01 us -> 2.7 us  [body(): lax.all_to_all(send, 'ep', split_axis=0, concat_axis=0, tiled=True)]
  transfers between devices with their start and end apart: 5 -> 11, of which waited for: 4 -> 7; matrix products, arithmetic and copies ran while one was open for 1% -> 0% of each run, Pallas kernels for 1% -> 0%
where the time goes in v2:
time: 185 us; the launch traced here: 182 us
  waiting for transfers between devices  96.6 us (52%)
  starting transfers between devices  64.9 us (35%)
  Pallas kernels  16.2 us (9%)
  local copies, waits for them, and re-layouts  3.66 us (2%)
    all_to_all x1, waiting for transfers between devices, body(): lax.all_to_all(results, 'ep', split_axis=0, concat_axis=0, tiled=True)  67.4 us
    ppermute x4, waiting for transfers between devices, gather_slices(): moving = lax.ppermute(moving, 'tp', onward)  25.2 us
    ppermute x4, starting transfers between devices, gather_slices(): moving = lax.ppermute(moving, 'tp', onward)  21 us
    all_to_all x1, starting transfers between devices, body(): lax.all_to_all(send, 'ep', split_axis=0, concat_axis=0, tiled=True)  19 us
    ppermute x4, starting transfers between devices, gather_slices(): pieces += [moving, lax.ppermute(moving, 'tp', partner)]  12.4 us
    pallas_call x1, Pallas kernels, body(): pl.pallas_call(functools.partial(ffn_kernel, 2), out_shape=buffer, in_spe...  9.84 us
    all_to_all x1, starting transfers between devices, body(): lax.all_to_all(results, 'ep', split_axis=0, concat_axis=0, tiled=True)  9.6 us
  transfers between devices with their start and end apart: 11, of which 7 were waited for; matrix products, arithmetic and copies ran while one was open for 0% of the time, Pallas kernels for 0%

profile of v2, /device:TPU:1, one launch (start us, length us, event | category | flops | bytes accessed | tf_op | source)
XLA Modules:
  0.0 181.9 jit_solution(6839848413355157090)
XLA Ops:
  0.0 3.2 %pack.1 = bf16[48,40,512]{2,1,0:T(8,128)(2,1)} custom-call(bf16[160,2048]{1,0:T(8,128)(2,1)} %tok_ref.3, s32[2,160]{1,0:T(2,128)} %bitcast.14), custom_call_target="tpu_custom_call" | custom-call | tf_op jit(solution)/shard_map/pack/pallas_call | solution.py:209
  3.2 0.0 copy-start.10
  3.3 19.0 %all-to-all-start = ((bf16[48,40,512]{2,1,0:T(8,128)(2,1)}), bf16[48,40,512]{2,1,0:T(8,128)(2,1)S(1)}, u32[]{:S(2)}, u32[]{:S(2)}) async-start(bf16[48,40,512]{2,1,0:T(8,128)(2,1)} %pack.1), calls=%async_computation | async-start | bytes 3932160 | tf_op jit(solution)/shard_map/all_to_all | solution.py:216
  22.3 2.9 %collective-permute-start = (bf16[96,2048]{1,0:T(8,128)(2,1)S(1)}, bf16[96,2048]{1,0:T(8,128)(2,1)S(1)}, u32[]{:S(2)}, u32[]{:S(2)}) collective-permute-start(bf16[96,2048]{1,0:T(8,128)(2,1)S(1)} %pad_maximum_fusion.1.refs_0_), channel_id=1, source_target_pairs={{0,1},{1,0},{2,3},{3,2},{4,5},{5,4},{6,7},{7,6},{8,9},{9,8},{10,11... | collective-permute-start | bytes 1179656 | tf_op jit(solution)/shard_map/ppermute | solution.py:185
  25.2 1.3 collective-permute-done.refs_1_
  26.5 0.1 pad_maximum_fusion
  26.6 5.1 %collective-permute-start.1 = (bf16[192,2048]{1,0:T(8,128)(2,1)S(1)}, bf16[192,2048]{1,0:T(8,128)(2,1)S(1)}, u32[]{:S(2)}, u32[]{:S(2)}) collective-permute-start(bf16[192,2048]{1,0:T(8,128)(2,1)S(1)} %pad_maximum_fusion), channel_id=1, source_target_pairs={{0,2},{1,15},{2,4},{3,1},{4,6},{5,3},{6,8},{7,5},{8,10},{9,7},{10,... | collective-permute-start | bytes 2359304 | tf_op jit(solution)/shard_map/ppermute | solution.py:192
  31.7 8.9 %collective-permute-done.1.refs_2_ = bf16[192,2048]{1,0:T(8,128)(2,1)S(1)} collective-permute-done((bf16[192,2048]{1,0:T(8,128)(2,1)S(1)}, bf16[192,2048]{1,0:T(8,128)(2,1)S(1)}, u32[]{:S(2)}, u32[]{:S(2)}) %collective-permute-start.1) | collective-permute-done | bytes 786464 | tf_op jit(solution)/shard_map/ppermute | solution.py:192
  40.6 5.3 %collective-permute-start.3 = (bf16[192,2048]{1,0:T(8,128)(2,1)S(1)}, bf16[192,2048]{1,0:T(8,128)(2,1)S(1)}, u32[]{:S(2)}, u32[]{:S(2)}) collective-permute-start(bf16[192,2048]{1,0:T(8,128)(2,1)S(1)} %collective-permute-done.1.refs_2_), channel_id=1, source_target_pairs={{0,2},{1,15},{2,4},{3,1},{4,6},{5,3},{6,8},{7,5},{8,10},{9,7},{10,... | collective-permute-start | bytes 2359304 | tf_op jit(solution)/shard_map/ppermute | solution.py:192
  45.9 8.9 %collective-permute-done.3.refs_4_ = bf16[192,2048]{1,0:T(8,128)(2,1)S(1)} collective-permute-done((bf16[192,2048]{1,0:T(8,128)(2,1)S(1)}, bf16[192,2048]{1,0:T(8,128)(2,1)S(1)}, u32[]{:S(2)}, u32[]{:S(2)}) %collective-permute-start.3) | collective-permute-done | bytes 786464 | tf_op jit(solution)/shard_map/ppermute | solution.py:192
  54.8 5.3 %collective-permute-start.5 = (bf16[192,2048]{1,0:T(8,128)(2,1)S(1)}, bf16[192,2048]{1,0:T(8,128)(2,1)S(1)}, u32[]{:S(2)}, u32[]{:S(2)}) collective-permute-start(bf16[192,2048]{1,0:T(8,128)(2,1)S(1)} %collective-permute-done.3.refs_4_), channel_id=1, source_target_pairs={{0,2},{1,15},{2,4},{3,1},{4,6},{5,3},{6,8},{7,5},{8,10},{9,7},{10,... | collective-permute-start | bytes 2359304 | tf_op jit(solution)/shard_map/ppermute | solution.py:192
  60.1 1.9 %collective-permute-start.2 = (bf16[192,2048]{1,0:T(8,128)(2,1)S(1)}, bf16[192,2048]{1,0:T(8,128)(2,1)S(1)}, u32[]{:S(2)}, u32[]{:S(2)}) collective-permute-start(bf16[192,2048]{1,0:T(8,128)(2,1)S(1)} %collective-permute-done.1.refs_2_), channel_id=1, source_target_pairs={{0,1},{1,0},{2,3},{3,2},{4,5},{5,4},{6,7},{7,6},{8,9},{9,8},{10,11... | collective-permute-start | bytes 2359304 | tf_op jit(solution)/shard_map/ppermute | solution.py:193
  62.1 2.4 %collective-permute-start.4 = (bf16[192,2048]{1,0:T(8,128)(2,1)S(1)}, bf16[192,2048]{1,0:T(8,128)(2,1)S(1)}, u32[]{:S(2)}, u32[]{:S(2)}) collective-permute-start(bf16[192,2048]{1,0:T(8,128)(2,1)S(1)} %collective-permute-done.3.refs_4_), channel_id=1, source_target_pairs={{0,1},{1,0},{2,3},{3,2},{4,5},{5,4},{6,7},{7,6},{8,9},{9,8},{10,11... | collective-permute-start | bytes 2359304 | tf_op jit(solution)/shard_map/ppermute | solution.py:193
  64.5 4.6 %collective-permute-done.5.refs_6_ = bf16[192,2048]{1,0:T(8,128)(2,1)S(1)} collective-permute-done((bf16[192,2048]{1,0:T(8,128)(2,1)S(1)}, bf16[192,2048]{1,0:T(8,128)(2,1)S(1)}, u32[]{:S(2)}, u32[]{:S(2)}) %collective-permute-start.5) | collective-permute-done | bytes 786464 | tf_op jit(solution)/shard_map/ppermute | solution.py:192
  69.1 5.3 %collective-permute-start.7 = (bf16[96,2048]{1,0:T(8,128)(2,1)S(1)}, bf16[96,2048]{1,0:T(8,128)(2,1)S(1)}, u32[]{:S(2)}, u32[]{:S(2)}) collective-permute-start(bf16[96,2048]{1,0:T(8,128)(2,1)S(1)} %slice.4), channel_id=1, source_target_pairs={{0,2},{1,15},{2,4},{3,1},{4,6},{5,3},{6,8},{7,5},{8,10},{9,7},{10,... | collective-permute-start | bytes 1179656 | tf_op jit(solution)/shard_map/ppermute | solution.py:192
  74.4 1.9 %collective-permute-start.6 = (bf16[192,2048]{1,0:T(8,128)(2,1)S(1)}, bf16[192,2048]{1,0:T(8,128)(2,1)S(1)}, u32[]{:S(2)}, u32[]{:S(2)}) collective-permute-start(bf16[192,2048]{1,0:T(8,128)(2,1)S(1)} %collective-permute-done.5.refs_6_), channel_id=1, source_target_pairs={{0,1},{1,0},{2,3},{3,2},{4,5},{5,4},{6,7},{7,6},{8,9},{9,8},{10,11... | collective-permute-start | bytes 2359304 | tf_op jit(solution)/shard_map/ppermute | solution.py:193
  76.3 2.8 %collective-permute-done.7.refs_8_ = bf16[96,2048]{1,0:T(8,128)(2,1)S(1)} collective-permute-done((bf16[96,2048]{1,0:T(8,128)(2,1)S(1)}, bf16[96,2048]{1,0:T(8,128)(2,1)S(1)}, u32[]{:S(2)}, u32[]{:S(2)}) %collective-permute-start.7) | collective-permute-done | bytes 393248 | tf_op jit(solution)/shard_map/ppermute | solution.py:192
  79.1 6.2 %collective-permute-start.8 = (bf16[96,2048]{1,0:T(8,128)(2,1)S(1)}, bf16[96,2048]{1,0:T(8,128)(2,1)S(1)}, u32[]{:S(2)}, u32[]{:S(2)}) collective-permute-start(bf16[96,2048]{1,0:T(8,128)(2,1)S(1)} %collective-permute-done.7.refs_8_), channel_id=1, source_target_pairs={{0,1},{1,0},{2,3},{3,2},{4,5},{5,4},{6,7},{7,6},{8,9},{9,8},{10,11... | collective-permute-start | bytes 1179656 | tf_op jit(solution)/shard_map/ppermute | solution.py:193
  85.4 0.8 copy-done.7
  86.2 0.3 copy-done.8
  86.5 1.0 copy-done.9
  87.4 2.7 %all-to-all-done.recv_ref = bf16[48,40,512]{2,1,0:T(8,128)(2,1)S(1)} async-done(((bf16[48,40,512]{2,1,0:T(8,128)(2,1)}), bf16[48,40,512]{2,1,0:T(8,128)(2,1)S(1)}, u32[]{:S(2)}, u32[]{:S(2)}) %all-to-all-start) | async-done | bytes 1966112 | tf_op jit(solution)/shard_map/all_to_all | solution.py:216
  90.1 1.3 copy-done.3
  91.4 9.8 %ffn.1 = bf16[48,40,512]{2,1,0:T(8,128)(2,1)} custom-call(bf16[48,40,512]{2,1,0:T(8,128)(2,1)} %copy-done.3, bf16[96,2048]{1,0:T(8,128)(2,1)S(1)} %pad_maximum_fusion.1.refs_0_, bf16[96,2048]{1,0:T(8,128)(2,1)S(1)} %collective-permute-done.refs_1_, bf16[192,2048]{1,0:T(8,128)(2,1)} %copy-done.5, bf16[192,2048]{1,0:T(8,128)(2,1)} %copy-done.7, ...), custom_call_target="tpu_custom_call" | custom-call | tf_op jit(solution)/shard_map/ffn/pallas_call | solution.py:220
  101.3 0.0 copy-start.14
  101.3 0.0 copy-start.13
  101.3 9.6 %all-to-all-start.1 = ((bf16[48,40,512]{2,1,0:T(8,128)(2,1)}), bf16[48,40,512]{2,1,0:T(8,128)(2,1)S(1)}, u32[]{:S(2)}, u32[]{:S(2)}) async-start(bf16[48,40,512]{2,1,0:T(8,128)(2,1)} %ffn.1), calls=%async_computation.1 | async-start | bytes 3932160 | tf_op jit(solution)/shard_map/all_to_all | solution.py:236
  111.0 0.1 copy.15.ids_ref
  111.1 0.1 copy.14
  111.2 0.1 broadcast_multiply_fusion.weight_ref
  111.3 67.4 %all-to-all-done.1.back_ref = bf16[48,40,512]{2,1,0:T(8,128)(2,1)S(1)} async-done(((bf16[48,40,512]{2,1,0:T(8,128)(2,1)}), bf16[48,40,512]{2,1,0:T(8,128)(2,1)S(1)}, u32[]{:S(2)}, u32[]{:S(2)}) %all-to-all-start.1) | async-done | bytes 1966112 | tf_op jit(solution)/shard_map/all_to_all | solution.py:236
  178.8 3.1 %mix.1 = bf16[160,2048]{1,0:T(8,128)(2,1)} custom-call(bf16[48,40,512]{2,1,0:T(8,128)(2,1)S(1)} %all-to-all-done.1.back_ref, bf16[160,2048]{1,0:T(8,128)(2,1)S(1)} %copy-done, s32[160,2]{1,0:T(8,128)S(1)} %copy.15.ids_ref, f32[160,2]{1,0:T(8,128)S(1)} %broadcast_multiply_fusion.weight_ref, f32[1,2048]{1,0:T(1,128)S(1)} %bitcast.6, f32[1,2048]{1,0:T(1,128)S(1)} %bitcast.7), custom_call_target="tpu_custom_call" | custom-call | tf_op jit(solution)/shard_map/mix/pallas_call | solution.py:239
  (33 shorter events, 0.2 us)
Async XLA Ops:
  3.2 19.0 %copy-start.10 = (bf16[1,32,2048]{2,1,0:T(8,128)(2,1)S(1)}, bf16[1,32,2048]{2,1,0:T(8,128)(2,1)}, u32[]{:S(2)}) copy-start(bf16[1,32,2048]{2,1,0:T(8,128)(2,1)} %param.15) | copy-start | bytes 393220
  3.2 19.0 %copy-start.11 = (bf16[1,32,2048]{2,1,0:T(8,128)(2,1)S(1)}, bf16[1,32,2048]{2,1,0:T(8,128)(2,1)}, u32[]{:S(2)}) copy-start(bf16[1,32,2048]{2,1,0:T(8,128)(2,1)} %param.14) | copy-start | bytes 393220
  3.2 19.0 %copy-start.12 = (bf16[1,32,2048]{2,1,0:T(8,128)(2,1)S(1)}, bf16[1,32,2048]{2,1,0:T(8,128)(2,1)}, u32[]{:S(2)}) copy-start(bf16[1,32,2048]{2,1,0:T(8,128)(2,1)} %param.13) | copy-start | bytes 393220
  3.3 86.9 %all-to-all-start = ((bf16[48,40,512]{2,1,0:T(8,128)(2,1)}), bf16[48,40,512]{2,1,0:T(8,128)(2,1)S(1)}, u32[]{:S(2)}, u32[]{:S(2)}) async-start(bf16[48,40,512]{2,1,0:T(8,128)(2,1)} %pack.1), calls=%async_computation | async-start | bytes 3932160 | tf_op jit(solution)/shard_map/all_to_all | solution.py:216
  22.3 4.2 %collective-permute-start = (bf16[96,2048]{1,0:T(8,128)(2,1)S(1)}, bf16[96,2048]{1,0:T(8,128)(2,1)S(1)}, u32[]{:S(2)}, u32[]{:S(2)}) collective-permute-start(bf16[96,2048]{1,0:T(8,128)(2,1)S(1)} %pad_maximum_fusion.1.refs_0_), channel_id=1, source_target_pairs={{0,1},{1,0},{2,3},{3,2},{4,5},{5,4},{6,7},{7,6},{8,9},{9,8},{10,11... | collective-permute-start | bytes 1179656 | tf_op jit(solution)/shard_map/ppermute | solution.py:185
  26.6 14.0 %collective-permute-start.1 = (bf16[192,2048]{1,0:T(8,128)(2,1)S(1)}, bf16[192,2048]{1,0:T(8,128)(2,1)S(1)}, u32[]{:S(2)}, u32[]{:S(2)}) collective-permute-start(bf16[192,2048]{1,0:T(8,128)(2,1)S(1)} %pad_maximum_fusion), channel_id=1, source_target_pairs={{0,2},{1,15},{2,4},{3,1},{4,6},{5,3},{6,8},{7,5},{8,10},{9,7},{10,... | collective-permute-start | bytes 2359304 | tf_op jit(solution)/shard_map/ppermute | solution.py:192
  40.6 44.7 %copy-start.5 = (bf16[192,2048]{1,0:T(8,128)(2,1)}, bf16[192,2048]{1,0:T(8,128)(2,1)S(1)}, u32[]{:S(2)}) copy-start(bf16[192,2048]{1,0:T(8,128)(2,1)S(1)} %collective-permute-done.1.refs_2_) | copy-start | bytes 2359300
  40.6 14.2 %collective-permute-start.3 = (bf16[192,2048]{1,0:T(8,128)(2,1)S(1)}, bf16[192,2048]{1,0:T(8,128)(2,1)S(1)}, u32[]{:S(2)}, u32[]{:S(2)}) collective-permute-start(bf16[192,2048]{1,0:T(8,128)(2,1)S(1)} %collective-permute-done.1.refs_2_), channel_id=1, source_target_pairs={{0,2},{1,15},{2,4},{3,1},{4,6},{5,3},{6,8},{7,5},{8,10},{9,7},{10,... | collective-permute-start | bytes 2359304 | tf_op jit(solution)/shard_map/ppermute | solution.py:192
  54.8 30.5 %copy-start.6 = (bf16[192,2048]{1,0:T(8,128)(2,1)}, bf16[192,2048]{1,0:T(8,128)(2,1)S(1)}, u32[]{:S(2)}) copy-start(bf16[192,2048]{1,0:T(8,128)(2,1)S(1)} %collective-permute-done.3.refs_4_) | copy-start | bytes 2359300
  54.8 14.2 %collective-permute-start.5 = (bf16[192,2048]{1,0:T(8,128)(2,1)S(1)}, bf16[192,2048]{1,0:T(8,128)(2,1)S(1)}, u32[]{:S(2)}, u32[]{:S(2)}) collective-permute-start(bf16[192,2048]{1,0:T(8,128)(2,1)S(1)} %collective-permute-done.3.refs_4_), channel_id=1, source_target_pairs={{0,2},{1,15},{2,4},{3,1},{4,6},{5,3},{6,8},{7,5},{8,10},{9,7},{10,... | collective-permute-start | bytes 2359304 | tf_op jit(solution)/shard_map/ppermute | solution.py:192
  60.1 25.1 %collective-permute-start.2 = (bf16[192,2048]{1,0:T(8,128)(2,1)S(1)}, bf16[192,2048]{1,0:T(8,128)(2,1)S(1)}, u32[]{:S(2)}, u32[]{:S(2)}) collective-permute-start(bf16[192,2048]{1,0:T(8,128)(2,1)S(1)} %collective-permute-done.1.refs_2_), channel_id=1, source_target_pairs={{0,1},{1,0},{2,3},{3,2},{4,5},{5,4},{6,7},{7,6},{8,9},{9,8},{10,11... | collective-permute-start | bytes 2359304 | tf_op jit(solution)/shard_map/ppermute | solution.py:193
  62.1 23.2 %collective-permute-start.4 = (bf16[192,2048]{1,0:T(8,128)(2,1)S(1)}, bf16[192,2048]{1,0:T(8,128)(2,1)S(1)}, u32[]{:S(2)}, u32[]{:S(2)}) collective-permute-start(bf16[192,2048]{1,0:T(8,128)(2,1)S(1)} %collective-permute-done.3.refs_4_), channel_id=1, source_target_pairs={{0,1},{1,0},{2,3},{3,2},{4,5},{5,4},{6,7},{7,6},{8,9},{9,8},{10,11... | collective-permute-start | bytes 2359304 | tf_op jit(solution)/shard_map/ppermute | solution.py:193
  69.1 16.3 %copy-start.4 = (bf16[192,2048]{1,0:T(8,128)(2,1)}, bf16[192,2048]{1,0:T(8,128)(2,1)S(1)}, u32[]{:S(2)}) copy-start(bf16[192,2048]{1,0:T(8,128)(2,1)S(1)} %collective-permute-done.5.refs_6_) | copy-start | bytes 2359300
  69.1 10.0 %collective-permute-start.7 = (bf16[96,2048]{1,0:T(8,128)(2,1)S(1)}, bf16[96,2048]{1,0:T(8,128)(2,1)S(1)}, u32[]{:S(2)}, u32[]{:S(2)}) collective-permute-start(bf16[96,2048]{1,0:T(8,128)(2,1)S(1)} %slice.4), channel_id=1, source_target_pairs={{0,2},{1,15},{2,4},{3,1},{4,6},{5,3},{6,8},{7,5},{8,10},{9,7},{10,... | collective-permute-start | bytes 1179656 | tf_op jit(solution)/shard_map/ppermute | solution.py:192
  74.4 10.9 %collective-permute-start.6 = (bf16[192,2048]{1,0:T(8,128)(2,1)S(1)}, bf16[192,2048]{1,0:T(8,128)(2,1)S(1)}, u32[]{:S(2)}, u32[]{:S(2)}) collective-permute-start(bf16[192,2048]{1,0:T(8,128)(2,1)S(1)} %collective-permute-done.5.refs_6_), channel_id=1, source_target_pairs={{0,1},{1,0},{2,3},{3,2},{4,5},{5,4},{6,7},{7,6},{8,9},{9,8},{10,11... | collective-permute-start | bytes 2359304 | tf_op jit(solution)/shard_map/ppermute | solution.py:193
  79.1 8.3 %collective-permute-start.8 = (bf16[96,2048]{1,0:T(8,128)(2,1)S(1)}, bf16[96,2048]{1,0:T(8,128)(2,1)S(1)}, u32[]{:S(2)}, u32[]{:S(2)}) collective-permute-start(bf16[96,2048]{1,0:T(8,128)(2,1)S(1)} %collective-permute-done.7.refs_8_), channel_id=1, source_target_pairs={{0,1},{1,0},{2,3},{3,2},{4,5},{5,4},{6,7},{7,6},{8,9},{9,8},{10,11... | collective-permute-start | bytes 1179656 | tf_op jit(solution)/shard_map/ppermute | solution.py:193
  85.3 0.9 copy-start.7
  85.3 1.1 copy-start.8
  86.5 1.0 copy-start.9
  90.1 1.3 copy-start.3
  101.3 9.7 %copy-start.14 = (s32[160,2]{0,1:T(2,128)S(1)}, s32[160,2]{0,1:T(2,128)}, u32[]{:S(2)}) copy-start(s32[160,2]{0,1:T(2,128)} %param.10) | copy-start | bytes 3844
  101.3 9.8 %copy-start.13 = (f32[160,2]{0,1:T(2,128)S(1)}, f32[160,2]{0,1:T(2,128)}, u32[]{:S(2)}) copy-start(f32[160,2]{0,1:T(2,128)} %param.12) | copy-start | bytes 3844
  101.3 9.9 %copy-start.15 = (f32[160]{0:T(256)S(1)}, f32[160]{0:T(256)}, u32[]{:S(2)}) copy-start(f32[160]{0:T(256)} %param.11) | copy-start | bytes 1924
  101.3 77.5 %copy-start = (bf16[160,2048]{1,0:T(8,128)(2,1)S(1)}, bf16[160,2048]{1,0:T(8,128)(2,1)}, u32[]{:S(2)}) copy-start(bf16[160,2048]{1,0:T(8,128)(2,1)} %tok_ref.3) | copy-start | bytes 1966084
  101.3 77.5 %copy-start.1 = (f32[2048]{0:T(1024)S(1)}, f32[2048]{0:T(1024)}, u32[]{:S(2)}) copy-start(f32[2048]{0:T(1024)} %param.16) | copy-start | bytes 24580
  101.3 77.5 %copy-start.2 = (f32[2048]{0:T(1024)S(1)}, f32[2048]{0:T(1024)}, u32[]{:S(2)}) copy-start(f32[2048]{0:T(1024)} %param.17) | copy-start | bytes 24580
  101.3 77.4 %all-to-all-start.1 = ((bf16[48,40,512]{2,1,0:T(8,128)(2,1)}), bf16[48,40,512]{2,1,0:T(8,128)(2,1)S(1)}, u32[]{:S(2)}, u32[]{:S(2)}) async-start(bf16[48,40,512]{2,1,0:T(8,128)(2,1)} %ffn.1), calls=%async_computation.1 | async-start | bytes 3932160 | tf_op jit(solution)/shard_map/all_to_all | solution.py:236

commit v3 on v2

--- a/solution.py
+++ b/solution.py
@@ -16,7 +16,7 @@
 REST = 2
 QUARTERS = 4
 SLICE = 32
-ROOM = 52 * 2**20
+ROOM = 50 * 2**20
 
 
 def dot(a, b):
@@ -70,32 +70,18 @@
         copy.wait()
 
 
-def ffn_kernel(chunks, recv_ref, *refs):
-    pieces, (out_ref, gate_ref, up_ref, down_ref, rows_ref, hidden_ref, staged_ref, sems, out_sems) = (
-        refs[:-9],
-        refs[-9:],
-    )
+def ffn_kernel(
+    chunks, recv_ref, gathered_ref, _, out_ref, weight_ref, rows_ref, hidden_ref, staged_ref, sems, out_sems
+):
     sources, _, width = recv_ref.shape
     heads, rests = sources * HEAD, sources * REST
-    hidden = gate_ref.shape[0]
-
+    slices, _, _, model_width = weight_ref.shape
+    size = slices // chunks
     waits = []
-    for piece in pieces:
-        for base in range(0, piece.shape[0], 3 * SLICE):
-            at = len(waits)
-            copies = [
-                pltpu.make_async_copy(
-                    piece.at[pl.ds(base + j * SLICE, SLICE), :],
-                    weight.at[pl.ds(at * SLICE, SLICE), :],
-                    sems.at[at, j],
-                )
-                for j, weight in enumerate((gate_ref, up_ref, down_ref))
-            ]
-            copies[0].start()
-            copies[1].start()
-            waits.append(copies)
-    for copies in waits:
-        copies[2].start()
+    for i in range(chunks):
+        part = pl.ds(i * size, size)
+        waits.append(pltpu.make_async_copy(gathered_ref.at[part], weight_ref.at[part], sems.at[i]))
+        waits[i].start()
 
     def pick(q):
         a = iota((rests, heads), 0)
@@ -111,22 +97,20 @@
         rows_ref[0:heads, cols] = recv_ref[:, q * HEAD : (q + 1) * HEAD, :].reshape(heads, width)
         rows_ref[heads:, cols] = dot(pick(q), rest).astype(BF16)
 
-    size = hidden // chunks
     for i in range(chunks):
-        for copies in waits[i * size // SLICE : (i + 1) * size // SLICE]:
-            copies[0].wait()
-            copies[1].wait()
+        waits[i].wait()
         part = slice(i * size, (i + 1) * size)
-        gate = dot_nt(rows_ref[...], gate_ref[part, :])
-        up = dot_nt(rows_ref[...], up_ref[part, :])
-        hidden_ref[:, part] = (gate / (1.0 + jnp.exp(-gate)) * up).astype(BF16)
-
-    for copies in waits:
-        copies[2].wait()
+        gate = dot_nt(rows_ref[...], weight_ref[part, 0].reshape(-1, model_width))
+        up = dot_nt(rows_ref[...], weight_ref[part, 1].reshape(-1, model_width))
+        hidden_ref[:, i * size * SLICE : (i + 1) * size * SLICE] = (
+            gate / (1.0 + jnp.exp(-gate)) * up
+        ).astype(BF16)
+
     rest = jnp.zeros((heads, width), F32)
     sent = []
     for q in range(QUARTERS):
-        result = dot(hidden_ref[...], down_ref[:, q * width : (q + 1) * width]).astype(BF16)
+        down = weight_ref[:, 2, :, q * width : (q + 1) * width].reshape(-1, width)
+        result = dot(hidden_ref[...], down).astype(BF16)
         staged_ref[q] = result[0:heads].reshape(sources, HEAD, width)
         sent.append(send_out(staged_ref, out_ref, out_sems, q))
         rest += dot(spread(q), result[heads:])
@@ -184,14 +168,15 @@
     onward = [(i, (i + 2 - 4 * (i % 2)) % size) for i in range(size)]
     other = lax.ppermute(own, "tp", partner)
     pieces = [own, other]
-    moving = jnp.concatenate([own, other], axis=0)
+    chains = [own, other]
     steps = size // 4
     for step in range(steps):
         if step == steps - 1:
-            moving = moving[: own.shape[0]]
-        moving = lax.ppermute(moving, "tp", onward)
-        pieces += [moving, lax.ppermute(moving, "tp", partner)]
-    return pieces
+            chains = chains[:1]
+        chains = [lax.ppermute(c, "tp", onward) for c in chains]
+        pieces += chains
+        pieces += [lax.ppermute(c, "tp", partner) for c in chains]
+    return jnp.concatenate(pieces, axis=0)
 
 
 def body(tokens, expert_ids, group_weight, expert_share, gate_w, up_w, down_w, out_gain, out_shift):
@@ -202,7 +187,7 @@
     hidden = gate_w.shape[1] * lax.axis_size("tp")
     buffer = jax.ShapeDtypeStruct((ep_size, block, width), BF16)
     vmem = pl.BlockSpec(memory_space=pltpu.VMEM)
-    hbm = pl.BlockSpec(memory_space=pltpu.HBM)
+    hbm = pl.BlockSpec(memory_space=pl.ANY)
     staged = pltpu.VMEM((QUARTERS + 1, ep_size, HEAD, width), BF16)
     staged_sems = pltpu.SemaphoreType.DMA((QUARTERS + 1,))
     limit = pltpu.CompilerParams(vmem_limit_bytes=32 * 2**20)
@@ -215,24 +200,25 @@
     )(tokens, expert_ids.T)
     received = lax.all_to_all(send, "ep", split_axis=0, concat_axis=0, tiled=True)
     own = jnp.concatenate([gate_w[0], up_w[0], down_w[0]], axis=0)
-    pieces = gather_slices(own)
+    gathered = gather_slices(own).reshape(-1, 3, SLICE, model_width)
     rows = ep_size * (HEAD + REST)
     results = pl.pallas_call(
         functools.partial(ffn_kernel, 2),
         out_shape=buffer,
-        in_specs=[vmem] + [hbm] * len(pieces),
+        in_specs=[vmem, hbm, hbm],
         out_specs=hbm,
-        scratch_shapes=[pltpu.VMEM((hidden, model_width), BF16)] * 3
-        + [
+        scratch_shapes=[
+            pltpu.VMEM(gathered.shape, BF16),
             pltpu.VMEM((rows, model_width), BF16),
             pltpu.VMEM((rows, hidden), BF16),
             staged,
-            pltpu.SemaphoreType.DMA((hidden // SLICE, 3)),
+            pltpu.SemaphoreType.DMA((2,)),
             staged_sems,
         ],
+        input_output_aliases={2: 0},
         compiler_params=pltpu.CompilerParams(vmem_limit_bytes=ROOM),
         name="ffn",
-    )(received, *pieces)
+    )(received, gathered, send)
     back = lax.all_to_all(results, "ep", split_axis=0, concat_axis=0, tiled=True)
     share_norm = expert_share / jnp.sum(expert_share, axis=1, keepdims=True)
     route_weight = group_weight[:, None] * share_norm

time: 185 us -> 184 us (level)
  waiting for transfers between devices: 96.6 us -> 75.8 us
  starting transfers between devices: 64.9 us -> 78.2 us
  local copies, waits for them, and re-layouts: 3.66 us -> 14 us
  Pallas kernels: 16.2 us -> 13.7 us
    ppermute x8 -> x14, waiting for transfers between devices: 25.2 us -> 5.8 us  [the longest x7 5.78 us: gather_slices(): chains = [lax.ppermute(c, 'tp', onward) for c in chains]]
    ppermute x8 -> x14, starting transfers between devices: 33.4 us -> 45.7 us  [the longest x7 24.7 us: gather_slices(): chains = [lax.ppermute(c, 'tp', onward) for c in chains]]
    unnamed x33 -> x36, local copies, waits for them, and re-layouts: 3.53 us -> 13.1 us
    pallas_call x1, Pallas kernels: 9.84 us -> 7.29 us  [body(): pl.pallas_call(functools.partial(ffn_kernel, 2), out_shape=buffer, in_spe...]
    all_to_all x1, waiting for transfers between devices: 2.7 us -> 0.45 us  [body(): lax.all_to_all(send, 'ep', split_axis=0, concat_axis=0, tiled=True)]
    all_to_all x1, starting transfers between devices: 9.6 us -> 11.7 us  [body(): lax.all_to_all(results, 'ep', split_axis=0, concat_axis=0, tiled=True)]
    all_to_all x1, waiting for transfers between devices: 67.4 us -> 69.6 us  [body(): lax.all_to_all(results, 'ep', split_axis=0, concat_axis=0, tiled=True)]
  transfers between devices with their start and end apart: 11 -> 17, of which waited for: 7 -> 5; matrix products, arithmetic and copies ran while one was open for 0% -> 8% of each run, Pallas kernels for 0% -> 0%
where the time goes in v3:
time: 184 us; the launch traced here: 182 us
  starting transfers between devices  78.2 us (42%)
  waiting for transfers between devices  75.8 us (41%)
  local copies, waits for them, and re-layouts  14 us (8%)
  Pallas kernels  13.7 us (7%)
    all_to_all x1, waiting for transfers between devices, body(): lax.all_to_all(results, 'ep', split_axis=0, concat_axis=0, tiled=True)  69.6 us
    ppermute x7, starting transfers between devices, gather_slices(): chains = [lax.ppermute(c, 'tp', onward) for c in chains]  24.7 us
    ppermute x7, starting transfers between devices, gather_slices(): pieces += [lax.ppermute(c, 'tp', partner) for c in chains]  21 us
    all_to_all x1, starting transfers between devices, body(): lax.all_to_all(send, 'ep', split_axis=0, concat_axis=0, tiled=True)  18.8 us
    unnamed x36, local copies, waits for them, and re-layouts  13.1 us
    all_to_all x1, starting transfers between devices, body(): lax.all_to_all(results, 'ep', split_axis=0, concat_axis=0, tiled=True)  11.7 us
    pallas_call x1, Pallas kernels, body(): pl.pallas_call(functools.partial(ffn_kernel, 2), out_shape=buffer, in_spe...  7.29 us
    ppermute x7, waiting for transfers between devices, gather_slices(): chains = [lax.ppermute(c, 'tp', onward) for c in chains]  5.78 us
  transfers between devices with their start and end apart: 17, of which 5 were waited for; matrix products, arithmetic and copies ran while one was open for 8% of the time, Pallas kernels for 0%

profile of v3, /device:TPU:1, one launch (start us, length us, event | category | flops | bytes accessed | tf_op | source)
XLA Modules:
  0.0 182.2 jit_solution(15824725120484932918)
XLA Ops:
  0.0 3.3 %pack.1._ = bf16[48,40,512]{2,1,0:T(8,128)(2,1)} custom-call(bf16[160,2048]{1,0:T(8,128)(2,1)} %tok_ref.3, s32[2,160]{1,0:T(2,128)} %bitcast.15), custom_call_target="tpu_custom_call" | custom-call | tf_op jit(solution)/shard_map/pack/pallas_call | solution.py:194
  3.3 18.8 %all-to-all-start = ((bf16[48,40,512]{2,1,0:T(8,128)(2,1)}), bf16[48,40,512]{2,1,0:T(8,128)(2,1)S(1)}, u32[]{:S(2)}, u32[]{:S(2)}) async-start(bf16[48,40,512]{2,1,0:T(8,128)(2,1)} %pack.1._), calls=%async_computation | async-start | bytes 3932160 | tf_op jit(solution)/shard_map/all_to_all | solution.py:201
  22.2 5.1 %collective-permute-start.1 = (bf16[96,2048]{1,0:T(8,128)(2,1)S(1)}, bf16[96,2048]{1,0:T(8,128)(2,1)S(1)}, u32[]{:S(2)}, u32[]{:S(2)}) collective-permute-start(bf16[96,2048]{1,0:T(8,128)(2,1)S(1)} %pad_maximum_fusion), channel_id=1, source_target_pairs={{0,2},{1,15},{2,4},{3,1},{4,6},{5,3},{6,8},{7,5},{8,10},{9,7},{10,... | collective-permute-start | bytes 1179656 | tf_op jit(solution)/shard_map/ppermute | solution.py:176
  27.3 1.9 %collective-permute-start = (bf16[96,2048]{1,0:T(8,128)(2,1)S(1)}, bf16[96,2048]{1,0:T(8,128)(2,1)S(1)}, u32[]{:S(2)}, u32[]{:S(2)}) collective-permute-start(bf16[96,2048]{1,0:T(8,128)(2,1)S(1)} %pad_maximum_fusion), channel_id=1, source_target_pairs={{0,1},{1,0},{2,3},{3,2},{4,5},{5,4},{6,7},{7,6},{8,9},{9,8},{10,11... | collective-permute-start | bytes 1179656 | tf_op jit(solution)/shard_map/ppermute | solution.py:169
  31.2 0.8 collective-permute-done.1
  32.0 4.2 %collective-permute-start.3 = (bf16[96,2048]{1,0:T(8,128)(2,1)S(1)}, bf16[96,2048]{1,0:T(8,128)(2,1)S(1)}, u32[]{:S(2)}, u32[]{:S(2)}) collective-permute-start(bf16[96,2048]{1,0:T(8,128)(2,1)S(1)} %collective-permute-done.1), channel_id=1, source_target_pairs={{0,1},{1,0},{2,3},{3,2},{4,5},{5,4},{6,7},{7,6},{8,9},{9,8},{10,11... | collective-permute-start | bytes 1179656 | tf_op jit(solution)/shard_map/ppermute | solution.py:178
  36.2 3.6 %collective-permute-start.5 = (bf16[96,2048]{1,0:T(8,128)(2,1)S(1)}, bf16[96,2048]{1,0:T(8,128)(2,1)S(1)}, u32[]{:S(2)}, u32[]{:S(2)}) collective-permute-start(bf16[96,2048]{1,0:T(8,128)(2,1)S(1)} %collective-permute-done.1), channel_id=1, source_target_pairs={{0,2},{1,15},{2,4},{3,1},{4,6},{5,3},{6,8},{7,5},{8,10},{9,7},{10,... | collective-permute-start | bytes 1179656 | tf_op jit(solution)/shard_map/ppermute | solution.py:176
  39.8 3.0 %collective-permute-start.2 = (bf16[96,2048]{1,0:T(8,128)(2,1)S(1)}, bf16[96,2048]{1,0:T(8,128)(2,1)S(1)}, u32[]{:S(2)}, u32[]{:S(2)}) collective-permute-start(bf16[96,2048]{1,0:T(8,128)(2,1)S(1)} %collective-permute-done), channel_id=1, source_target_pairs={{0,2},{1,15},{2,4},{3,1},{4,6},{5,3},{6,8},{7,5},{8,10},{9,7},{10,... | collective-permute-start | bytes 1179656 | tf_op jit(solution)/shard_map/ppermute | solution.py:176
  43.6 0.8 constant_dynamic-update-slice_fusion.13
  44.4 4.8 %collective-permute-done.2 = bf16[96,2048]{1,0:T(8,128)(2,1)S(1)} collective-permute-done((bf16[96,2048]{1,0:T(8,128)(2,1)S(1)}, bf16[96,2048]{1,0:T(8,128)(2,1)S(1)}, u32[]{:S(2)}, u32[]{:S(2)}) %collective-permute-start.2) | collective-permute-done | bytes 393248 | tf_op jit(solution)/shard_map/ppermute | solution.py:176
  49.2 4.0 %collective-permute-start.4 = (bf16[96,2048]{1,0:T(8,128)(2,1)S(1)}, bf16[96,2048]{1,0:T(8,128)(2,1)S(1)}, u32[]{:S(2)}, u32[]{:S(2)}) collective-permute-start(bf16[96,2048]{1,0:T(8,128)(2,1)S(1)} %collective-permute-done.2), channel_id=1, source_target_pairs={{0,1},{1,0},{2,3},{3,2},{4,5},{5,4},{6,7},{7,6},{8,9},{9,8},{10,11... | collective-permute-start | bytes 1179656 | tf_op jit(solution)/shard_map/ppermute | solution.py:178
  53.2 2.8 %collective-permute-start.6 = (bf16[96,2048]{1,0:T(8,128)(2,1)S(1)}, bf16[96,2048]{1,0:T(8,128)(2,1)S(1)}, u32[]{:S(2)}, u32[]{:S(2)}) collective-permute-start(bf16[96,2048]{1,0:T(8,128)(2,1)S(1)} %collective-permute-done.2), channel_id=1, source_target_pairs={{0,2},{1,15},{2,4},{3,1},{4,6},{5,3},{6,8},{7,5},{8,10},{9,7},{10,... | collective-permute-start | bytes 1179656 | tf_op jit(solution)/shard_map/ppermute | solution.py:176
  56.0 1.9 %collective-permute-start.7 = (bf16[96,2048]{1,0:T(8,128)(2,1)S(1)}, bf16[96,2048]{1,0:T(8,128)(2,1)S(1)}, u32[]{:S(2)}, u32[]{:S(2)}) collective-permute-start(bf16[96,2048]{1,0:T(8,128)(2,1)S(1)} %collective-permute-done.5), channel_id=1, source_target_pairs={{0,1},{1,0},{2,3},{3,2},{4,5},{5,4},{6,7},{7,6},{8,9},{9,8},{10,11... | collective-permute-start | bytes 1179656 | tf_op jit(solution)/shard_map/ppermute | solution.py:178
  57.9 4.0 %collective-permute-start.9 = (bf16[96,2048]{1,0:T(8,128)(2,1)S(1)}, bf16[96,2048]{1,0:T(8,128)(2,1)S(1)}, u32[]{:S(2)}, u32[]{:S(2)}) collective-permute-start(bf16[96,2048]{1,0:T(8,128)(2,1)S(1)} %collective-permute-done.5), channel_id=1, source_target_pairs={{0,2},{1,15},{2,4},{3,1},{4,6},{5,3},{6,8},{7,5},{8,10},{9,7},{10,... | collective-permute-start | bytes 1179656 | tf_op jit(solution)/shard_map/ppermute | solution.py:176
  62.7 0.8 constant_dynamic-update-slice_fusion.11
  63.5 2.5 %collective-permute-start.8 = (bf16[96,2048]{1,0:T(8,128)(2,1)S(1)}, bf16[96,2048]{1,0:T(8,128)(2,1)S(1)}, u32[]{:S(2)}, u32[]{:S(2)}) collective-permute-start(bf16[96,2048]{1,0:T(8,128)(2,1)S(1)} %collective-permute-done.6), channel_id=1, source_target_pairs={{0,1},{1,0},{2,3},{3,2},{4,5},{5,4},{6,7},{7,6},{8,9},{9,8},{10,11... | collective-permute-start | bytes 1179656 | tf_op jit(solution)/shard_map/ppermute | solution.py:178
  66.0 2.7 %collective-permute-start.10 = (bf16[96,2048]{1,0:T(8,128)(2,1)S(1)}, bf16[96,2048]{1,0:T(8,128)(2,1)S(1)}, u32[]{:S(2)}, u32[]{:S(2)}) collective-permute-start(bf16[96,2048]{1,0:T(8,128)(2,1)S(1)} %collective-permute-done.6), channel_id=1, source_target_pairs={{0,2},{1,15},{2,4},{3,1},{4,6},{5,3},{6,8},{7,5},{8,10},{9,7},{10,... | collective-permute-start | bytes 1179656 | tf_op jit(solution)/shard_map/ppermute | solution.py:176
  68.7 2.5 %collective-permute-start.11 = (bf16[96,2048]{1,0:T(8,128)(2,1)S(1)}, bf16[96,2048]{1,0:T(8,128)(2,1)S(1)}, u32[]{:S(2)}, u32[]{:S(2)}) collective-permute-start(bf16[96,2048]{1,0:T(8,128)(2,1)S(1)} %collective-permute-done.9), channel_id=1, source_target_pairs={{0,1},{1,0},{2,3},{3,2},{4,5},{5,4},{6,7},{7,6},{8,9},{9,8},{10,11... | collective-permute-start | bytes 1179656 | tf_op jit(solution)/shard_map/ppermute | solution.py:178
  71.2 3.5 %collective-permute-start.13 = (bf16[96,2048]{1,0:T(8,128)(2,1)S(1)}, bf16[96,2048]{1,0:T(8,128)(2,1)S(1)}, u32[]{:S(2)}, u32[]{:S(2)}) collective-permute-start(bf16[96,2048]{1,0:T(8,128)(2,1)S(1)} %collective-permute-done.9), channel_id=1, source_target_pairs={{0,2},{1,15},{2,4},{3,1},{4,6},{5,3},{6,8},{7,5},{8,10},{9,7},{10,... | collective-permute-start | bytes 1179656 | tf_op jit(solution)/shard_map/ppermute | solution.py:176
  75.5 0.8 constant_dynamic-update-slice_fusion.9
  76.3 0.8 constant_dynamic-update-slice_fusion.8
  77.8 2.7 %collective-permute-start.12 = (bf16[96,2048]{1,0:T(8,128)(2,1)S(1)}, bf16[96,2048]{1,0:T(8,128)(2,1)S(1)}, u32[]{:S(2)}, u32[]{:S(2)}) collective-permute-start(bf16[96,2048]{1,0:T(8,128)(2,1)S(1)} %collective-permute-done.10), channel_id=1, source_target_pairs={{0,1},{1,0},{2,3},{3,2},{4,5},{5,4},{6,7},{7,6},{8,9},{9,8},{10,11... | collective-permute-start | bytes 1179656 | tf_op jit(solution)/shard_map/ppermute | solution.py:178
  80.7 3.3 %collective-permute-start.14 = (bf16[96,2048]{1,0:T(8,128)(2,1)S(1)}, bf16[96,2048]{1,0:T(8,128)(2,1)S(1)}, u32[]{:S(2)}, u32[]{:S(2)}) collective-permute-start(bf16[96,2048]{1,0:T(8,128)(2,1)S(1)} %collective-permute-done.13), channel_id=1, source_target_pairs={{0,1},{1,0},{2,3},{3,2},{4,5},{5,4},{6,7},{7,6},{8,9},{9,8},{10,11... | collective-permute-start | bytes 1179656 | tf_op jit(solution)/shard_map/ppermute | solution.py:178
  85.6 0.8 constant_dynamic-update-slice_fusion.4
  86.4 0.8 constant_dynamic-update-slice_fusion.3
  87.2 0.8 constant_dynamic-update-slice_fusion.2
  88.0 0.8 constant_dynamic-update-slice_fusion.1
  88.8 0.8 constant_dynamic-update-slice_fusion
  90.1 7.3 %ffn.1 = bf16[48,40,512]{2,1,0:T(8,128)(2,1)} custom-call(bf16[48,40,512]{2,1,0:T(8,128)(2,1)S(1)} %all-to-all-done.recv_ref, bf16[16,3,32,2048]{3,2,1,0:T(8,128)(2,1)} %bitcast.4.gathered_ref, bf16[48,40,512]{2,1,0:T(8,128)(2,1)} %pack.1._), custom_call_target="tpu_custom_call", output_to_operand_aliasing={{}: (2, {})} | custom-call | tf_op jit(solution)/shard_map/ffn/pallas_call | solution.py:205
  97.3 11.7 %all-to-all-start.1 = ((bf16[48,40,512]{2,1,0:T(8,128)(2,1)}), bf16[48,40,512]{2,1,0:T(8,128)(2,1)S(1)}, u32[]{:S(2)}, u32[]{:S(2)}) async-start(bf16[48,40,512]{2,1,0:T(8,128)(2,1)} %ffn.1), calls=%async_computation.1 | async-start | bytes 3932160 | tf_op jit(solution)/shard_map/all_to_all | solution.py:222
  109.5 69.6 %all-to-all-done.1.back_ref = bf16[48,40,512]{2,1,0:T(8,128)(2,1)S(1)} async-done(((bf16[48,40,512]{2,1,0:T(8,128)(2,1)}), bf16[48,40,512]{2,1,0:T(8,128)(2,1)S(1)}, u32[]{:S(2)}, u32[]{:S(2)}) %all-to-all-start.1) | async-done | bytes 1966112 | tf_op jit(solution)/shard_map/all_to_all | solution.py:222
  179.1 3.1 %mix.1 = bf16[160,2048]{1,0:T(8,128)(2,1)} custom-call(bf16[48,40,512]{2,1,0:T(8,128)(2,1)S(1)} %all-to-all-done.1.back_ref, bf16[160,2048]{1,0:T(8,128)(2,1)S(1)} %copy-done, s32[160,2]{1,0:T(8,128)S(1)} %copy.16.ids_ref, f32[160,2]{1,0:T(8,128)S(1)} %broadcast_multiply_fusion.weight_ref, f32[1,2048]{1,0:T(1,128)S(1)} %bitcast.10, f32[1,2048]{1,0:T(1,128)S(1)} %bitcast.11), custom_call_target="tpu_custom_call" | custom-call | tf_op jit(solution)/shard_map/mix/pallas_call | solution.py:225
  (47 shorter events, 7.6 us)
Async XLA Ops:
  0.0 22.1 %copy-start.3 = (bf16[1,32,2048]{2,1,0:T(8,128)(2,1)S(1)}, bf16[1,32,2048]{2,1,0:T(8,128)(2,1)}, u32[]{:S(2)}) copy-start(bf16[1,32,2048]{2,1,0:T(8,128)(2,1)} %param.13) | copy-start | bytes 393220
  0.0 22.1 %copy-start.4 = (bf16[1,32,2048]{2,1,0:T(8,128)(2,1)S(1)}, bf16[1,32,2048]{2,1,0:T(8,128)(2,1)}, u32[]{:S(2)}) copy-start(bf16[1,32,2048]{2,1,0:T(8,128)(2,1)} %param.14) | copy-start | bytes 393220
  0.0 22.2 %copy-start.5 = (bf16[1,32,2048]{2,1,0:T(8,128)(2,1)S(1)}, bf16[1,32,2048]{2,1,0:T(8,128)(2,1)}, u32[]{:S(2)}) copy-start(bf16[1,32,2048]{2,1,0:T(8,128)(2,1)} %param.15) | copy-start | bytes 393220
  3.3 86.7 %all-to-all-start = ((bf16[48,40,512]{2,1,0:T(8,128)(2,1)}), bf16[48,40,512]{2,1,0:T(8,128)(2,1)S(1)}, u32[]{:S(2)}, u32[]{:S(2)}) async-start(bf16[48,40,512]{2,1,0:T(8,128)(2,1)} %pack.1._), calls=%async_computation | async-start | bytes 3932160 | tf_op jit(solution)/shard_map/all_to_all | solution.py:201
  22.2 9.8 %collective-permute-start.1 = (bf16[96,2048]{1,0:T(8,128)(2,1)S(1)}, bf16[96,2048]{1,0:T(8,128)(2,1)S(1)}, u32[]{:S(2)}, u32[]{:S(2)}) collective-permute-start(bf16[96,2048]{1,0:T(8,128)(2,1)S(1)} %pad_maximum_fusion), channel_id=1, source_target_pairs={{0,2},{1,15},{2,4},{3,1},{4,6},{5,3},{6,8},{7,5},{8,10},{9,7},{10,... | collective-permute-start | bytes 1179656 | tf_op jit(solution)/shard_map/ppermute | solution.py:176
  27.3 12.5 %collective-permute-start = (bf16[96,2048]{1,0:T(8,128)(2,1)S(1)}, bf16[96,2048]{1,0:T(8,128)(2,1)S(1)}, u32[]{:S(2)}, u32[]{:S(2)}) collective-permute-start(bf16[96,2048]{1,0:T(8,128)(2,1)S(1)} %pad_maximum_fusion), channel_id=1, source_target_pairs={{0,1},{1,0},{2,3},{3,2},{4,5},{5,4},{6,7},{7,6},{8,9},{9,8},{10,11... | collective-permute-start | bytes 1179656 | tf_op jit(solution)/shard_map/ppermute | solution.py:169
  32.0 30.7 %collective-permute-start.3 = (bf16[96,2048]{1,0:T(8,128)(2,1)S(1)}, bf16[96,2048]{1,0:T(8,128)(2,1)S(1)}, u32[]{:S(2)}, u32[]{:S(2)}) collective-permute-start(bf16[96,2048]{1,0:T(8,128)(2,1)S(1)} %collective-permute-done.1), channel_id=1, source_target_pairs={{0,1},{1,0},{2,3},{3,2},{4,5},{5,4},{6,7},{7,6},{8,9},{9,8},{10,11... | collective-permute-start | bytes 1179656 | tf_op jit(solution)/shard_map/ppermute | solution.py:178
  36.2 19.8 %collective-permute-start.5 = (bf16[96,2048]{1,0:T(8,128)(2,1)S(1)}, bf16[96,2048]{1,0:T(8,128)(2,1)S(1)}, u32[]{:S(2)}, u32[]{:S(2)}) collective-permute-start(bf16[96,2048]{1,0:T(8,128)(2,1)S(1)} %collective-permute-done.1), channel_id=1, source_target_pairs={{0,2},{1,15},{2,4},{3,1},{4,6},{5,3},{6,8},{7,5},{8,10},{9,7},{10,... | collective-permute-start | bytes 1179656 | tf_op jit(solution)/shard_map/ppermute | solution.py:176
  39.8 9.4 %collective-permute-start.2 = (bf16[96,2048]{1,0:T(8,128)(2,1)S(1)}, bf16[96,2048]{1,0:T(8,128)(2,1)S(1)}, u32[]{:S(2)}, u32[]{:S(2)}) collective-permute-start(bf16[96,2048]{1,0:T(8,128)(2,1)S(1)} %collective-permute-done), channel_id=1, source_target_pairs={{0,2},{1,15},{2,4},{3,1},{4,6},{5,3},{6,8},{7,5},{8,10},{9,7},{10,... | collective-permute-start | bytes 1179656 | tf_op jit(solution)/shard_map/ppermute | solution.py:176
  49.2 22.0 %collective-permute-start.4 = (bf16[96,2048]{1,0:T(8,128)(2,1)S(1)}, bf16[96,2048]{1,0:T(8,128)(2,1)S(1)}, u32[]{:S(2)}, u32[]{:S(2)}) collective-permute-start(bf16[96,2048]{1,0:T(8,128)(2,1)S(1)} %collective-permute-done.2), channel_id=1, source_target_pairs={{0,1},{1,0},{2,3},{3,2},{4,5},{5,4},{6,7},{7,6},{8,9},{9,8},{10,11... | collective-permute-start | bytes 1179656 | tf_op jit(solution)/shard_map/ppermute | solution.py:178
  53.2 10.3 %collective-permute-start.6 = (bf16[96,2048]{1,0:T(8,128)(2,1)S(1)}, bf16[96,2048]{1,0:T(8,128)(2,1)S(1)}, u32[]{:S(2)}, u32[]{:S(2)}) collective-permute-start(bf16[96,2048]{1,0:T(8,128)(2,1)S(1)} %collective-permute-done.2), channel_id=1, source_target_pairs={{0,2},{1,15},{2,4},{3,1},{4,6},{5,3},{6,8},{7,5},{8,10},{9,7},{10,... | collective-permute-start | bytes 1179656 | tf_op jit(solution)/shard_map/ppermute | solution.py:176
  56.0 21.1 %collective-permute-start.7 = (bf16[96,2048]{1,0:T(8,128)(2,1)S(1)}, bf16[96,2048]{1,0:T(8,128)(2,1)S(1)}, u32[]{:S(2)}, u32[]{:S(2)}) collective-permute-start(bf16[96,2048]{1,0:T(8,128)(2,1)S(1)} %collective-permute-done.5), channel_id=1, source_target_pairs={{0,1},{1,0},{2,3},{3,2},{4,5},{5,4},{6,7},{7,6},{8,9},{9,8},{10,11... | collective-permute-start | bytes 1179656 | tf_op jit(solution)/shard_map/ppermute | solution.py:178
  57.9 10.8 %collective-permute-start.9 = (bf16[96,2048]{1,0:T(8,128)(2,1)S(1)}, bf16[96,2048]{1,0:T(8,128)(2,1)S(1)}, u32[]{:S(2)}, u32[]{:S(2)}) collective-permute-start(bf16[96,2048]{1,0:T(8,128)(2,1)S(1)} %collective-permute-done.5), channel_id=1, source_target_pairs={{0,2},{1,15},{2,4},{3,1},{4,6},{5,3},{6,8},{7,5},{8,10},{9,7},{10,... | collective-permute-start | bytes 1179656 | tf_op jit(solution)/shard_map/ppermute | solution.py:176
  63.5 20.5 %collective-permute-start.8 = (bf16[96,2048]{1,0:T(8,128)(2,1)S(1)}, bf16[96,2048]{1,0:T(8,128)(2,1)S(1)}, u32[]{:S(2)}, u32[]{:S(2)}) collective-permute-start(bf16[96,2048]{1,0:T(8,128)(2,1)S(1)} %collective-permute-done.6), channel_id=1, source_target_pairs={{0,1},{1,0},{2,3},{3,2},{4,5},{5,4},{6,7},{7,6},{8,9},{9,8},{10,11... | collective-permute-start | bytes 1179656 | tf_op jit(solution)/shard_map/ppermute | solution.py:178
  66.0 11.8 %collective-permute-start.10 = (bf16[96,2048]{1,0:T(8,128)(2,1)S(1)}, bf16[96,2048]{1,0:T(8,128)(2,1)S(1)}, u32[]{:S(2)}, u32[]{:S(2)}) collective-permute-start(bf16[96,2048]{1,0:T(8,128)(2,1)S(1)} %collective-permute-done.6), channel_id=1, source_target_pairs={{0,2},{1,15},{2,4},{3,1},{4,6},{5,3},{6,8},{7,5},{8,10},{9,7},{10,... | collective-permute-start | bytes 1179656 | tf_op jit(solution)/shard_map/ppermute | solution.py:176
  68.7 17.6 %collective-permute-start.11 = (bf16[96,2048]{1,0:T(8,128)(2,1)S(1)}, bf16[96,2048]{1,0:T(8,128)(2,1)S(1)}, u32[]{:S(2)}, u32[]{:S(2)}) collective-permute-start(bf16[96,2048]{1,0:T(8,128)(2,1)S(1)} %collective-permute-done.9), channel_id=1, source_target_pairs={{0,1},{1,0},{2,3},{3,2},{4,5},{5,4},{6,7},{7,6},{8,9},{9,8},{10,11... | collective-permute-start | bytes 1179656 | tf_op jit(solution)/shard_map/ppermute | solution.py:178
  71.2 9.5 %collective-permute-start.13 = (bf16[96,2048]{1,0:T(8,128)(2,1)S(1)}, bf16[96,2048]{1,0:T(8,128)(2,1)S(1)}, u32[]{:S(2)}, u32[]{:S(2)}) collective-permute-start(bf16[96,2048]{1,0:T(8,128)(2,1)S(1)} %collective-permute-done.9), channel_id=1, source_target_pairs={{0,2},{1,15},{2,4},{3,1},{4,6},{5,3},{6,8},{7,5},{8,10},{9,7},{10,... | collective-permute-start | bytes 1179656 | tf_op jit(solution)/shard_map/ppermute | solution.py:176
  77.8 9.3 %collective-permute-start.12 = (bf16[96,2048]{1,0:T(8,128)(2,1)S(1)}, bf16[96,2048]{1,0:T(8,128)(2,1)S(1)}, u32[]{:S(2)}, u32[]{:S(2)}) collective-permute-start(bf16[96,2048]{1,0:T(8,128)(2,1)S(1)} %collective-permute-done.10), channel_id=1, source_target_pairs={{0,1},{1,0},{2,3},{3,2},{4,5},{5,4},{6,7},{7,6},{8,9},{9,8},{10,11... | collective-permute-start | bytes 1179656 | tf_op jit(solution)/shard_map/ppermute | solution.py:178
  80.7 8.1 %collective-permute-start.14 = (bf16[96,2048]{1,0:T(8,128)(2,1)S(1)}, bf16[96,2048]{1,0:T(8,128)(2,1)S(1)}, u32[]{:S(2)}, u32[]{:S(2)}) collective-permute-start(bf16[96,2048]{1,0:T(8,128)(2,1)S(1)} %collective-permute-done.13), channel_id=1, source_target_pairs={{0,1},{1,0},{2,3},{3,2},{4,5},{5,4},{6,7},{7,6},{8,9},{9,8},{10,11... | collective-permute-start | bytes 1179656 | tf_op jit(solution)/shard_map/ppermute | solution.py:178
  90.0 19.1 %copy-start.7 = (s32[160,2]{0,1:T(2,128)S(1)}, s32[160,2]{0,1:T(2,128)}, u32[]{:S(2)}) copy-start(s32[160,2]{0,1:T(2,128)} %param.10) | copy-start | bytes 3844
  90.0 19.2 %copy-start.6 = (f32[160,2]{0,1:T(2,128)S(1)}, f32[160,2]{0,1:T(2,128)}, u32[]{:S(2)}) copy-start(f32[160,2]{0,1:T(2,128)} %param.12) | copy-start | bytes 3844
  90.0 19.4 %copy-start.8 = (f32[160]{0:T(256)S(1)}, f32[160]{0:T(256)}, u32[]{:S(2)}) copy-start(f32[160]{0:T(256)} %param.11) | copy-start | bytes 1924
  90.0 89.0 %copy-start = (bf16[160,2048]{1,0:T(8,128)(2,1)S(1)}, bf16[160,2048]{1,0:T(8,128)(2,1)}, u32[]{:S(2)}) copy-start(bf16[160,2048]{1,0:T(8,128)(2,1)} %tok_ref.3) | copy-start | bytes 1966084
  90.0 89.0 %copy-start.1 = (f32[2048]{0:T(1024)S(1)}, f32[2048]{0:T(1024)}, u32[]{:S(2)}) copy-start(f32[2048]{0:T(1024)} %param.16) | copy-start | bytes 24580
  90.0 89.0 %copy-start.2 = (f32[2048]{0:T(1024)S(1)}, f32[2048]{0:T(1024)}, u32[]{:S(2)}) copy-start(f32[2048]{0:T(1024)} %param.17) | copy-start | bytes 24580
  97.3 81.7 %all-to-all-start.1 = ((bf16[48,40,512]{2,1,0:T(8,128)(2,1)}), bf16[48,40,512]{2,1,0:T(8,128)(2,1)S(1)}, u32[]{:S(2)}, u32[]{:S(2)}) async-start(bf16[48,40,512]{2,1,0:T(8,128)(2,1)} %ffn.1), calls=%async_computation.1 | async-start | bytes 3932160 | tf_op jit(solution)/shard_map/all_to_all | solution.py:222

commit v4 on v3

--- a/solution.py
+++ b/solution.py
@@ -17,6 +17,7 @@
 QUARTERS = 4
 SLICE = 32
 ROOM = 50 * 2**20
+LATE = 1
 
 
 def dot(a, b):
@@ -71,17 +72,19 @@
 
 
 def ffn_kernel(
-    chunks, recv_ref, gathered_ref, _, out_ref, weight_ref, rows_ref, hidden_ref, staged_ref, sems, out_sems
+    chunks, recv_ref, _, *refs
 ):
+    pieces, (out_ref, weight_ref, rows_ref, hidden_ref, staged_ref, sems, out_sems) = refs[:-7], refs[-7:]
     sources, _, width = recv_ref.shape
     heads, rests = sources * HEAD, sources * REST
     slices, _, _, model_width = weight_ref.shape
     size = slices // chunks
-    waits = []
-    for i in range(chunks):
-        part = pl.ds(i * size, size)
-        waits.append(pltpu.make_async_copy(gathered_ref.at[part], weight_ref.at[part], sems.at[i]))
-        waits[i].start()
+    waits, at = [], 0
+    for n, piece in enumerate(pieces):
+        copy = pltpu.make_async_copy(piece, weight_ref.at[pl.ds(at, piece.shape[0])], sems.at[n])
+        copy.start()
+        at += piece.shape[0]
+        waits.append((at, copy))
 
     def pick(q):
         a = iota((rests, heads), 0)
@@ -98,7 +101,9 @@
         rows_ref[heads:, cols] = dot(pick(q), rest).astype(BF16)
 
     for i in range(chunks):
-        waits[i].wait()
+        for end, copy in waits:
+            if i * size < end <= (i + 1) * size:
+                copy.wait()
         part = slice(i * size, (i + 1) * size)
         gate = dot_nt(rows_ref[...], weight_ref[part, 0].reshape(-1, model_width))
         up = dot_nt(rows_ref[...], weight_ref[part, 1].reshape(-1, model_width))
@@ -118,6 +123,31 @@
     sent.append(send_out(staged_ref, out_ref, out_sems, QUARTERS))
     for copy in sent:
         copy.wait()
+
+
+def collect_kernel(late_ref, own_ref, *refs):
+    pieces, (out_ref, staged_ref, in_sems, out_sems) = refs[:-4], refs[-4:]
+    half = len(pieces) // 2
+
+    def load(piece, n):
+        return pltpu.make_async_copy(piece, staged_ref.at[n], in_sems.at[n])
+
+    def store(n):
+        return pltpu.make_async_copy(staged_ref.at[n], out_ref.at[n], out_sems.at[n])
+
+    load(own_ref, 0).start()
+    for late, chosen in ((0, pieces[:half]), (1, pieces[half:])):
+
+        @pl.when(late_ref[0] == late)
+        def _():
+            for n, piece in enumerate(chosen):
+                load(piece, n + 1).start()
+
+    for n in range(half + 1):
+        load(own_ref, n).wait()
+        store(n).start()
+    for n in range(half + 1):
+        store(n).wait()
 
 
 def mix_kernel(back_ref, tok_ref, ids_ref, weight_ref, gain_ref, shift_ref, out_ref, sum_ref):
@@ -162,21 +192,14 @@
     out_ref[...] = (center * lax.rsqrt(variance + norm_eps) * gain_ref[...] + shift_ref[...]).astype(BF16)
 
 
-def gather_slices(own):
+def ring(own, core):
     size = lax.axis_size("tp")
-    partner = [(i, i ^ 1) for i in range(size)]
-    onward = [(i, (i + 2 - 4 * (i % 2)) % size) for i in range(size)]
-    other = lax.ppermute(own, "tp", partner)
-    pieces = [own, other]
-    chains = [own, other]
-    steps = size // 4
-    for step in range(steps):
-        if step == steps - 1:
-            chains = chains[:1]
-        chains = [lax.ppermute(c, "tp", onward) for c in chains]
-        pieces += chains
-        pieces += [lax.ppermute(c, "tp", partner) for c in chains]
-    return jnp.concatenate(pieces, axis=0)
+
+    def move(x, chips):
+        return lax.ppermute(x, "tp", [(i, (i + 2 * chips) % size) for i in range(core, size, 2)])
+
+    up, down = move(own, 2), move(own, -2)
+    return [up, down, move(own, 1), move(own, -1), move(up, 2), move(up, 1), move(down, -1)]
 
 
 def body(tokens, expert_ids, group_weight, expert_share, gate_w, up_w, down_w, out_gain, out_shift):
@@ -198,27 +221,48 @@
         scratch_shapes=[staged, staged_sems],
         name="pack",
     )(tokens, expert_ids.T)
+    late = (lax.axis_index("tp") % 2 == LATE).astype(jnp.int32).reshape(1)
+    own = jnp.concatenate([gate_w[0], up_w[0], down_w[0]], axis=0)
+    late_pieces = ring(own, LATE)
+    smem = pl.BlockSpec(memory_space=pltpu.SMEM)
+    send, late_pieces = lax.optimization_barrier((send, late_pieces))
     received = lax.all_to_all(send, "ep", split_axis=0, concat_axis=0, tiled=True)
-    own = jnp.concatenate([gate_w[0], up_w[0], down_w[0]], axis=0)
-    gathered = gather_slices(own).reshape(-1, 3, SLICE, model_width)
+    own, send = lax.optimization_barrier((own, send))
+    early_pieces = ring(own, 1 - LATE)
+    count = len(early_pieces) + 1
+    slices = (count,) + own.shape
+    collected = pl.pallas_call(
+        collect_kernel,
+        out_shape=jax.ShapeDtypeStruct(slices, BF16),
+        in_specs=[smem] + [hbm] * (2 * count - 1),
+        out_specs=hbm,
+        scratch_shapes=[
+            pltpu.VMEM(slices, BF16),
+            pltpu.SemaphoreType.DMA((count,)),
+            pltpu.SemaphoreType.DMA((count,)),
+        ],
+        name="collect",
+    )(late, own, *early_pieces, *late_pieces)
+    other = lax.ppermute(collected, "tp", [(i, i ^ 1) for i in range(lax.axis_size("tp"))])
+    pieces = [p.reshape(count, 3, SLICE, model_width) for p in (collected, other)]
     rows = ep_size * (HEAD + REST)
     results = pl.pallas_call(
         functools.partial(ffn_kernel, 2),
         out_shape=buffer,
-        in_specs=[vmem, hbm, hbm],
+        in_specs=[vmem] + [hbm] * (len(pieces) + 1),
         out_specs=hbm,
         scratch_shapes=[
-            pltpu.VMEM(gathered.shape, BF16),
+            pltpu.VMEM((hidden // SLICE, 3, SLICE, model_width), BF16),
             pltpu.VMEM((rows, model_width), BF16),
             pltpu.VMEM((rows, hidden), BF16),
             staged,
-            pltpu.SemaphoreType.DMA((2,)),
+            pltpu.SemaphoreType.DMA((len(pieces),)),
             staged_sems,
         ],
-        input_output_aliases={2: 0},
+        input_output_aliases={1: 0},
         compiler_params=pltpu.CompilerParams(vmem_limit_bytes=ROOM),
         name="ffn",
-    )(received, gathered, send)
+    )(received, send, *pieces)
     back = lax.all_to_all(results, "ep", split_axis=0, concat_axis=0, tiled=True)
     share_norm = expert_share / jnp.sum(expert_share, axis=1, keepdims=True)
     route_weight = group_weight[:, None] * share_norm

time: 184 us -> 178 us (0.967)
  waiting for transfers between devices: 75.8 us -> 89 us
  local copies, waits for them, and re-layouts: 14 us -> 1.89 us
  starting transfers between devices: 78.2 us -> 68.8 us
  Pallas kernels: 13.7 us -> 16.4 us
    all_to_all x1, waiting for transfers between devices: 0.45 us -> 20.5 us  [body(): lax.all_to_all(send, 'ep', split_axis=0, concat_axis=0, tiled=True)]
    all_to_all x1, waiting for transfers between devices: 69.6 us -> 56.9 us  [body(): lax.all_to_all(results, 'ep', split_axis=0, concat_axis=0, tiled=True)]
    ppermute x15, starting transfers between devices: 47.7 us -> 35.3 us  [the longest x14 33.4 us: move(): lax.ppermute(x, 'tp', [(i, (i + 2 * chips) % size) for i in range(core, s...]
    unnamed x36 -> x35, local copies, waits for them, and re-layouts: 13.1 us -> 1.78 us
    all_to_all x1, starting transfers between devices: 18.8 us -> 27.4 us  [body(): lax.all_to_all(send, 'ep', split_axis=0, concat_axis=0, tiled=True)]
    ppermute x15, waiting for transfers between devices: 5.8 us -> 11.6 us  [the longest x1 5.97 us: body(): lax.ppermute(collected, 'tp', [(i, i ^ 1) for i in range(lax.axis_size('t...]
    all_to_all x1, starting transfers between devices: 11.7 us -> 6.15 us  [body(): lax.all_to_all(results, 'ep', split_axis=0, concat_axis=0, tiled=True)]
    pallas_call x0 -> x1, Pallas kernels: none -> 2.76 us  [body(): pl.pallas_call(collect_kernel, out_shape=jax.ShapeDtypeStruct(slices, BF1...]
  transfers between devices with their start and end apart: 17 -> 17, of which waited for: 5 -> 5; matrix products, arithmetic and copies ran while one was open for 8% -> 0% of each run, Pallas kernels for 0% -> 3%
where the time goes in v4:
time: 178 us
  waiting for transfers between devices  89 us (50%)
  starting transfers between devices  68.8 us (39%)
  Pallas kernels  16.4 us (9%)
  local copies, waits for them, and re-layouts  1.89 us (1%)
    all_to_all x1, waiting for transfers between devices, body(): lax.all_to_all(results, 'ep', split_axis=0, concat_axis=0, tiled=True)  56.9 us
    ppermute x14, starting transfers between devices, move(): lax.ppermute(x, 'tp', [(i, (i + 2 * chips) % size) for i in range(core, s...  33.4 us
    all_to_all x1, starting transfers between devices, body(): lax.all_to_all(send, 'ep', split_axis=0, concat_axis=0, tiled=True)  27.4 us
    all_to_all x1, waiting for transfers between devices, body(): lax.all_to_all(send, 'ep', split_axis=0, concat_axis=0, tiled=True)  20.5 us
    pallas_call x1, Pallas kernels, body(): pl.pallas_call(functools.partial(ffn_kernel, 2), out_shape=buffer, in_spe...  7.3 us
    all_to_all x1, starting transfers between devices, body(): lax.all_to_all(results, 'ep', split_axis=0, concat_axis=0, tiled=True)  6.15 us
    ppermute x1, waiting for transfers between devices, body(): lax.ppermute(collected, 'tp', [(i, i ^ 1) for i in range(lax.axis_size('t...  5.97 us
    ppermute x14, waiting for transfers between devices, move(): lax.ppermute(x, 'tp', [(i, (i + 2 * chips) % size) for i in range(core, s...  5.58 us
  transfers between devices with their start and end apart: 17, of which 5 were waited for; matrix products, arithmetic and copies ran while one was open for 0% of the time, Pallas kernels for 3%

profile of v4, /device:TPU:1, one launch (start us, length us, event | category | flops | bytes accessed | tf_op | source)
XLA Modules:
  0.0 177.7 jit_solution(8025372051785230218)
XLA Ops:
  0.0 1.1 pad_maximum_fusion.own_ref
  1.1 5.0 %collective-permute-start = (bf16[96,2048]{1,0:T(8,128)(2,1)S(1)}, bf16[96,2048]{1,0:T(8,128)(2,1)S(1)}, u32[]{:S(2)}, u32[]{:S(2)}) collective-permute-start(bf16[96,2048]{1,0:T(8,128)(2,1)S(1)} %pad_maximum_fusion.own_ref), channel_id=1, source_target_pairs={{1,5},{3,7},{5,9},{7,11},{9,13},{11,15},{13,1},{15,3},{17,21},{19,... | collective-permute-start | bytes 1179656 | tf_op jit(solution)/shard_map/ppermute | solution.py:199
  6.1 3.6 %collective-permute-start.1 = (bf16[96,2048]{1,0:T(8,128)(2,1)S(1)}, bf16[96,2048]{1,0:T(8,128)(2,1)S(1)}, u32[]{:S(2)}, u32[]{:S(2)}) collective-permute-start(bf16[96,2048]{1,0:T(8,128)(2,1)S(1)} %pad_maximum_fusion.own_ref), channel_id=1, source_target_pairs={{1,13},{3,15},{5,1},{7,3},{9,5},{11,7},{13,9},{15,11},{17,29},{19,... | collective-permute-start | bytes 1179656 | tf_op jit(solution)/shard_map/ppermute | solution.py:199
  9.7 2.8 %collective-permute-start.2 = (bf16[96,2048]{1,0:T(8,128)(2,1)S(1)}, bf16[96,2048]{1,0:T(8,128)(2,1)S(1)}, u32[]{:S(2)}, u32[]{:S(2)}) collective-permute-start(bf16[96,2048]{1,0:T(8,128)(2,1)S(1)} %pad_maximum_fusion.own_ref), channel_id=1, source_target_pairs={{1,3},{3,5},{5,7},{7,9},{9,11},{11,13},{13,15},{15,1},{17,19},{19,... | collective-permute-start | bytes 1179656 | tf_op jit(solution)/shard_map/ppermute | solution.py:199
  12.5 3.7 %collective-permute-start.3 = (bf16[96,2048]{1,0:T(8,128)(2,1)S(1)}, bf16[96,2048]{1,0:T(8,128)(2,1)S(1)}, u32[]{:S(2)}, u32[]{:S(2)}) collective-permute-start(bf16[96,2048]{1,0:T(8,128)(2,1)S(1)} %pad_maximum_fusion.own_ref), channel_id=1, source_target_pairs={{1,15},{3,1},{5,3},{7,5},{9,7},{11,9},{13,11},{15,13},{17,31},{19,... | collective-permute-start | bytes 1179656 | tf_op jit(solution)/shard_map/ppermute | solution.py:199
  16.2 4.0 %collective-permute-start.4 = (bf16[96,2048]{1,0:T(8,128)(2,1)S(1)}, bf16[96,2048]{1,0:T(8,128)(2,1)S(1)}, u32[]{:S(2)}, u32[]{:S(2)}) collective-permute-start(bf16[96,2048]{1,0:T(8,128)(2,1)S(1)} %collective-permute-done.refs_7_), channel_id=1, source_target_pairs={{1,5},{3,7},{5,9},{7,11},{9,13},{11,15},{13,1},{15,3},{17,21},{19,... | collective-permute-start | bytes 1179656 | tf_op jit(solution)/shard_map/ppermute | solution.py:199
  20.3 2.8 %collective-permute-start.5 = (bf16[96,2048]{1,0:T(8,128)(2,1)S(1)}, bf16[96,2048]{1,0:T(8,128)(2,1)S(1)}, u32[]{:S(2)}, u32[]{:S(2)}) collective-permute-start(bf16[96,2048]{1,0:T(8,128)(2,1)S(1)} %collective-permute-done.refs_7_), channel_id=1, source_target_pairs={{1,3},{3,5},{5,7},{7,9},{9,11},{11,13},{13,15},{15,1},{17,19},{19,... | collective-permute-start | bytes 1179656 | tf_op jit(solution)/shard_map/ppermute | solution.py:199
  23.1 3.7 %collective-permute-start.6 = (bf16[96,2048]{1,0:T(8,128)(2,1)S(1)}, bf16[96,2048]{1,0:T(8,128)(2,1)S(1)}, u32[]{:S(2)}, u32[]{:S(2)}) collective-permute-start(bf16[96,2048]{1,0:T(8,128)(2,1)S(1)} %collective-permute-done.1.refs_8_), channel_id=1, source_target_pairs={{1,15},{3,1},{5,3},{7,5},{9,7},{11,9},{13,11},{15,13},{17,31},{19,... | collective-permute-start | bytes 1179656 | tf_op jit(solution)/shard_map/ppermute | solution.py:199
  26.8 3.2 %pack.1._ = bf16[48,40,512]{2,1,0:T(8,128)(2,1)} custom-call(bf16[160,2048]{1,0:T(8,128)(2,1)} %tok_ref.3, s32[2,160]{1,0:T(2,128)} %bitcast.15), custom_call_target="tpu_custom_call" | custom-call | tf_op jit(solution)/shard_map/pack/pallas_call | solution.py:217
  30.0 1.1 collective-permute-done.4.refs_11_
  31.1 4.5 %collective-permute-done.5.refs_12_ = bf16[96,2048]{1,0:T(8,128)(2,1)S(1)} collective-permute-done((bf16[96,2048]{1,0:T(8,128)(2,1)S(1)}, bf16[96,2048]{1,0:T(8,128)(2,1)S(1)}, u32[]{:S(2)}, u32[]{:S(2)}) %collective-permute-start.5) | collective-permute-done | bytes 393248 | tf_op jit(solution)/shard_map/ppermute | solution.py:199
  35.6 0.8 copy-done.9
  36.4 0.1 copy-done.10
  36.5 27.4 %all-to-all-start = ((bf16[48,40,512]{2,1,0:T(8,128)(2,1)}), bf16[48,40,512]{2,1,0:T(8,128)(2,1)S(1)}, u32[]{:S(2)}, u32[]{:S(2)}) async-start(bf16[48,40,512]{2,1,0:T(8,128)(2,1)} %pack.1._), calls=%async_computation | async-start | bytes 3932160 | tf_op jit(solution)/shard_map/all_to_all | solution.py:229
  63.9 0.7 collective-permute-start.7
  64.6 0.7 collective-permute-start.8
  65.3 0.7 collective-permute-start.10
  66.0 1.4 collective-permute-start.9
  67.5 1.4 collective-permute-start.11
  68.9 1.4 collective-permute-start.12
  70.3 1.4 collective-permute-start.13
  71.8 0.7 copy-done.13
  72.5 2.8 %collect.1 = bf16[8,96,2048]{2,1,0:T(8,128)(2,1)} custom-call(s32[1]{0:T(128)} %bitcast.4.late_ref, bf16[96,2048]{1,0:T(8,128)(2,1)} %copy-done.3, bf16[96,2048]{1,0:T(8,128)(2,1)} %copy-done.11, bf16[96,2048]{1,0:T(8,128)(2,1)} %copy-done.12, bf16[96,2048]{1,0:T(8,128)(2,1)} %collective-permute-done.9.refs_2_, bf16[96,2048]{1,0:T(8,128)(2,1)} %copy-done.13, ...), custom_call_target="tpu_custom_call" | custom-call | tf_op jit(solution)/shard_map/collect/pallas_call | solution.py:234
  75.3 1.9 %collective-permute-start.14 = (bf16[8,96,2048]{2,1,0:T(8,128)(2,1)}, bf16[8,96,2048]{2,1,0:T(8,128)(2,1)}, u32[]{:S(2)}, u32[]{:S(2)}) collective-permute-start(bf16[8,96,2048]{2,1,0:T(8,128)(2,1)} %collect.1), channel_id=1, source_target_pairs={{0,1},{1,0},{2,3},{3,2},{4,5},{5,4},{6,7},{7,6},{8,9},{9,8},{10,11... | collective-permute-start | bytes 9437192 | tf_op jit(solution)/shard_map/ppermute | solution.py:246
  77.2 6.0 %collective-permute-done.14 = bf16[8,96,2048]{2,1,0:T(8,128)(2,1)} collective-permute-done((bf16[8,96,2048]{2,1,0:T(8,128)(2,1)}, bf16[8,96,2048]{2,1,0:T(8,128)(2,1)}, u32[]{:S(2)}, u32[]{:S(2)}) %collective-permute-start.14) | collective-permute-done | bytes 3145760 | tf_op jit(solution)/shard_map/ppermute | solution.py:246
  83.2 20.5 %all-to-all-done.recv_ref = bf16[48,40,512]{2,1,0:T(8,128)(2,1)S(1)} async-done(((bf16[48,40,512]{2,1,0:T(8,128)(2,1)}), bf16[48,40,512]{2,1,0:T(8,128)(2,1)S(1)}, u32[]{:S(2)}, u32[]{:S(2)}) %all-to-all-start) | async-done | bytes 1966112 | tf_op jit(solution)/shard_map/all_to_all | solution.py:229
  103.7 7.3 %ffn.1 = bf16[48,40,512]{2,1,0:T(8,128)(2,1)} custom-call(bf16[48,40,512]{2,1,0:T(8,128)(2,1)S(1)} %all-to-all-done.recv_ref, bf16[48,40,512]{2,1,0:T(8,128)(2,1)} %pack.1._, bf16[8,3,32,2048]{3,2,1,0:T(8,128)(2,1)} %bitcast.11, bf16[8,3,32,2048]{3,2,1,0:T(8,128)(2,1)} %bitcast.6.refs_1_), custom_call_target="tpu_custom_call", output_to_operand_aliasing={{}: (1, {})} | custom-call | tf_op jit(solution)/shard_map/ffn/pallas_call | solution.py:249
  111.1 6.1 %all-to-all-start.1 = ((bf16[48,40,512]{2,1,0:T(8,128)(2,1)}), bf16[48,40,512]{2,1,0:T(8,128)(2,1)S(1)}, u32[]{:S(2)}, u32[]{:S(2)}) async-start(bf16[48,40,512]{2,1,0:T(8,128)(2,1)} %ffn.1), calls=%async_computation.1 | async-start | bytes 3932160 | tf_op jit(solution)/shard_map/all_to_all | solution.py:266
  117.2 0.1 copy.16.ids_ref
  117.4 0.1 copy.15
  117.6 56.9 %all-to-all-done.1.back_ref = bf16[48,40,512]{2,1,0:T(8,128)(2,1)S(1)} async-done(((bf16[48,40,512]{2,1,0:T(8,128)(2,1)}), bf16[48,40,512]{2,1,0:T(8,128)(2,1)S(1)}, u32[]{:S(2)}, u32[]{:S(2)}) %all-to-all-start.1) | async-done | bytes 1966112 | tf_op jit(solution)/shard_map/all_to_all | solution.py:266
  174.6 3.1 %mix.1 = bf16[160,2048]{1,0:T(8,128)(2,1)} custom-call(bf16[48,40,512]{2,1,0:T(8,128)(2,1)S(1)} %all-to-all-done.1.back_ref, bf16[160,2048]{1,0:T(8,128)(2,1)S(1)} %copy-done, s32[160,2]{1,0:T(8,128)S(1)} %copy.16.ids_ref, f32[160,2]{1,0:T(8,128)S(1)} %broadcast_multiply_fusion.weight_ref, f32[1,2048]{1,0:T(1,128)S(1)} %bitcast.9, f32[1,2048]{1,0:T(1,128)S(1)} %bitcast.10), custom_call_target="tpu_custom_call" | custom-call | tf_op jit(solution)/shard_map/mix/pallas_call | solution.py:269
  (46 shorter events, 0.2 us)
Async XLA Ops:
  1.1 65.0 %copy-start.3 = (bf16[96,2048]{1,0:T(8,128)(2,1)}, bf16[96,2048]{1,0:T(8,128)(2,1)S(1)}, u32[]{:S(2)}) copy-start(bf16[96,2048]{1,0:T(8,128)(2,1)S(1)} %pad_maximum_fusion.own_ref) | copy-start | bytes 1179652
  1.1 15.1 %collective-permute-start = (bf16[96,2048]{1,0:T(8,128)(2,1)S(1)}, bf16[96,2048]{1,0:T(8,128)(2,1)S(1)}, u32[]{:S(2)}, u32[]{:S(2)}) collective-permute-start(bf16[96,2048]{1,0:T(8,128)(2,1)S(1)} %pad_maximum_fusion.own_ref), channel_id=1, source_target_pairs={{1,5},{3,7},{5,9},{7,11},{9,13},{11,15},{13,1},{15,3},{17,21},{19,... | collective-permute-start | bytes 1179656 | tf_op jit(solution)/shard_map/ppermute | solution.py:199
  6.1 17.0 %collective-permute-start.1 = (bf16[96,2048]{1,0:T(8,128)(2,1)S(1)}, bf16[96,2048]{1,0:T(8,128)(2,1)S(1)}, u32[]{:S(2)}, u32[]{:S(2)}) collective-permute-start(bf16[96,2048]{1,0:T(8,128)(2,1)S(1)} %pad_maximum_fusion.own_ref), channel_id=1, source_target_pairs={{1,13},{3,15},{5,1},{7,3},{9,5},{11,7},{13,9},{15,11},{17,29},{19,... | collective-permute-start | bytes 1179656 | tf_op jit(solution)/shard_map/ppermute | solution.py:199
  9.7 20.3 %collective-permute-start.2 = (bf16[96,2048]{1,0:T(8,128)(2,1)S(1)}, bf16[96,2048]{1,0:T(8,128)(2,1)S(1)}, u32[]{:S(2)}, u32[]{:S(2)}) collective-permute-start(bf16[96,2048]{1,0:T(8,128)(2,1)S(1)} %pad_maximum_fusion.own_ref), channel_id=1, source_target_pairs={{1,3},{3,5},{5,7},{7,9},{9,11},{11,13},{13,15},{15,1},{17,19},{19,... | collective-permute-start | bytes 1179656 | tf_op jit(solution)/shard_map/ppermute | solution.py:199
  12.5 17.5 %collective-permute-start.3 = (bf16[96,2048]{1,0:T(8,128)(2,1)S(1)}, bf16[96,2048]{1,0:T(8,128)(2,1)S(1)}, u32[]{:S(2)}, u32[]{:S(2)}) collective-permute-start(bf16[96,2048]{1,0:T(8,128)(2,1)S(1)} %pad_maximum_fusion.own_ref), channel_id=1, source_target_pairs={{1,15},{3,1},{5,3},{7,5},{9,7},{11,9},{13,11},{15,13},{17,31},{19,... | collective-permute-start | bytes 1179656 | tf_op jit(solution)/shard_map/ppermute | solution.py:199
  16.2 20.3 %copy-start.4 = (bf16[96,2048]{1,0:T(8,128)(2,1)}, bf16[96,2048]{1,0:T(8,128)(2,1)S(1)}, u32[]{:S(2)}) copy-start(bf16[96,2048]{1,0:T(8,128)(2,1)S(1)} %collective-permute-done.refs_7_) | copy-start | bytes 1179652
  16.2 14.9 %collective-permute-start.4 = (bf16[96,2048]{1,0:T(8,128)(2,1)S(1)}, bf16[96,2048]{1,0:T(8,128)(2,1)S(1)}, u32[]{:S(2)}, u32[]{:S(2)}) collective-permute-start(bf16[96,2048]{1,0:T(8,128)(2,1)S(1)} %collective-permute-done.refs_7_), channel_id=1, source_target_pairs={{1,5},{3,7},{5,9},{7,11},{9,13},{11,15},{13,1},{15,3},{17,21},{19,... | collective-permute-start | bytes 1179656 | tf_op jit(solution)/shard_map/ppermute | solution.py:199
  20.3 15.3 %collective-permute-start.5 = (bf16[96,2048]{1,0:T(8,128)(2,1)S(1)}, bf16[96,2048]{1,0:T(8,128)(2,1)S(1)}, u32[]{:S(2)}, u32[]{:S(2)}) collective-permute-start(bf16[96,2048]{1,0:T(8,128)(2,1)S(1)} %collective-permute-done.refs_7_), channel_id=1, source_target_pairs={{1,3},{3,5},{5,7},{7,9},{9,11},{11,13},{13,15},{15,1},{17,19},{19,... | collective-permute-start | bytes 1179656 | tf_op jit(solution)/shard_map/ppermute | solution.py:199
  23.1 13.4 %copy-start.5 = (bf16[96,2048]{1,0:T(8,128)(2,1)}, bf16[96,2048]{1,0:T(8,128)(2,1)S(1)}, u32[]{:S(2)}) copy-start(bf16[96,2048]{1,0:T(8,128)(2,1)S(1)} %collective-permute-done.1.refs_8_) | copy-start | bytes 1179652
  23.1 12.5 %collective-permute-start.6 = (bf16[96,2048]{1,0:T(8,128)(2,1)S(1)}, bf16[96,2048]{1,0:T(8,128)(2,1)S(1)}, u32[]{:S(2)}, u32[]{:S(2)}) collective-permute-start(bf16[96,2048]{1,0:T(8,128)(2,1)S(1)} %collective-permute-done.1.refs_8_), channel_id=1, source_target_pairs={{1,15},{3,1},{5,3},{7,5},{9,7},{11,9},{13,11},{15,13},{17,31},{19,... | collective-permute-start | bytes 1179656 | tf_op jit(solution)/shard_map/ppermute | solution.py:199
  30.0 6.5 %copy-start.6 = (bf16[96,2048]{1,0:T(8,128)(2,1)}, bf16[96,2048]{1,0:T(8,128)(2,1)S(1)}, u32[]{:S(2)}) copy-start(bf16[96,2048]{1,0:T(8,128)(2,1)S(1)} %collective-permute-done.2.refs_9_) | copy-start | bytes 1179652
  30.0 5.6 %copy-start.7 = (bf16[96,2048]{1,0:T(8,128)(2,1)}, bf16[96,2048]{1,0:T(8,128)(2,1)S(1)}, u32[]{:S(2)}) copy-start(bf16[96,2048]{1,0:T(8,128)(2,1)S(1)} %collective-permute-done.3.refs_10_) | copy-start | bytes 1179652
  31.1 4.5 %copy-start.8 = (bf16[96,2048]{1,0:T(8,128)(2,1)}, bf16[96,2048]{1,0:T(8,128)(2,1)S(1)}, u32[]{:S(2)}) copy-start(bf16[96,2048]{1,0:T(8,128)(2,1)S(1)} %collective-permute-done.4.refs_11_) | copy-start | bytes 1179652
  35.6 0.9 copy-start.10
  36.5 67.2 %all-to-all-start = ((bf16[48,40,512]{2,1,0:T(8,128)(2,1)}), bf16[48,40,512]{2,1,0:T(8,128)(2,1)S(1)}, u32[]{:S(2)}, u32[]{:S(2)}) async-start(bf16[48,40,512]{2,1,0:T(8,128)(2,1)} %pack.1._), calls=%async_computation | async-start | bytes 3932160 | tf_op jit(solution)/shard_map/all_to_all | solution.py:229
  63.9 3.5 %collective-permute-start.7 = (bf16[96,2048]{1,0:T(8,128)(2,1)S(1)}, bf16[96,2048]{1,0:T(8,128)(2,1)S(1)}, u32[]{:S(2)}, u32[]{:S(2)}) collective-permute-start(bf16[96,2048]{1,0:T(8,128)(2,1)S(1)} %pad_maximum_fusion.own_ref), channel_id=1, source_target_pairs={{0,4},{2,6},{4,8},{6,10},{8,12},{10,14},{12,0},{14,2},{16,20},{18,... | collective-permute-start | bytes 1179656 | tf_op jit(solution)/shard_map/ppermute | solution.py:199
  64.6 5.6 %collective-permute-start.8 = (bf16[96,2048]{1,0:T(8,128)(2,1)S(1)}, bf16[96,2048]{1,0:T(8,128)(2,1)S(1)}, u32[]{:S(2)}, u32[]{:S(2)}) collective-permute-start(bf16[96,2048]{1,0:T(8,128)(2,1)S(1)} %pad_maximum_fusion.own_ref), channel_id=1, source_target_pairs={{0,12},{2,14},{4,0},{6,2},{8,4},{10,6},{12,8},{14,10},{16,28},{18,... | collective-permute-start | bytes 1179656 | tf_op jit(solution)/shard_map/ppermute | solution.py:199
  65.3 6.4 %collective-permute-start.10 = (bf16[96,2048]{1,0:T(8,128)(2,1)S(1)}, bf16[96,2048]{1,0:T(8,128)(2,1)S(1)}, u32[]{:S(2)}, u32[]{:S(2)}) collective-permute-start(bf16[96,2048]{1,0:T(8,128)(2,1)S(1)} %pad_maximum_fusion.own_ref), channel_id=1, source_target_pairs={{0,14},{2,0},{4,2},{6,4},{8,6},{10,8},{12,10},{14,12},{16,30},{18,... | collective-permute-start | bytes 1179656 | tf_op jit(solution)/shard_map/ppermute | solution.py:199
  66.0 5.7 %collective-permute-start.9 = (bf16[96,2048]{1,0:T(8,128)(2,1)S(1)}, bf16[96,2048]{1,0:T(8,128)(2,1)}, u32[]{:S(2)}, u32[]{:S(2)}) collective-permute-start(bf16[96,2048]{1,0:T(8,128)(2,1)S(1)} %pad_maximum_fusion.own_ref), channel_id=1, source_target_pairs={{0,2},{2,4},{4,6},{6,8},{8,10},{10,12},{12,14},{14,0},{16,18},{18,... | collective-permute-start | bytes 1179656 | tf_op jit(solution)/shard_map/ppermute | solution.py:199
  67.5 4.3 %copy-start.11 = (bf16[96,2048]{1,0:T(8,128)(2,1)}, bf16[96,2048]{1,0:T(8,128)(2,1)S(1)}, u32[]{:S(2)}) copy-start(bf16[96,2048]{1,0:T(8,128)(2,1)S(1)} %collective-permute-done.7.refs_0_) | copy-start | bytes 1179652
  67.5 4.3 %collective-permute-start.11 = (bf16[96,2048]{1,0:T(8,128)(2,1)S(1)}, bf16[96,2048]{1,0:T(8,128)(2,1)}, u32[]{:S(2)}, u32[]{:S(2)}) collective-permute-start(bf16[96,2048]{1,0:T(8,128)(2,1)S(1)} %collective-permute-done.7.refs_0_), channel_id=1, source_target_pairs={{0,4},{2,6},{4,8},{6,10},{8,12},{10,14},{12,0},{14,2},{16,20},{18,... | collective-permute-start | bytes 1179656 | tf_op jit(solution)/shard_map/ppermute | solution.py:199
  68.9 2.9 %collective-permute-start.12 = (bf16[96,2048]{1,0:T(8,128)(2,1)S(1)}, bf16[96,2048]{1,0:T(8,128)(2,1)}, u32[]{:S(2)}, u32[]{:S(2)}) collective-permute-start(bf16[96,2048]{1,0:T(8,128)(2,1)S(1)} %collective-permute-done.7.refs_0_), channel_id=1, source_target_pairs={{0,2},{2,4},{4,6},{6,8},{8,10},{10,12},{12,14},{14,0},{16,18},{18,... | collective-permute-start | bytes 1179656 | tf_op jit(solution)/shard_map/ppermute | solution.py:199
  70.3 1.5 copy-start.12
  70.3 1.5 collective-permute-start.13
  75.3 7.9 %collective-permute-start.14 = (bf16[8,96,2048]{2,1,0:T(8,128)(2,1)}, bf16[8,96,2048]{2,1,0:T(8,128)(2,1)}, u32[]{:S(2)}, u32[]{:S(2)}) collective-permute-start(bf16[8,96,2048]{2,1,0:T(8,128)(2,1)} %collect.1), channel_id=1, source_target_pairs={{0,1},{1,0},{2,3},{3,2},{4,5},{5,4},{6,7},{7,6},{8,9},{9,8},{10,11... | collective-permute-start | bytes 9437192 | tf_op jit(solution)/shard_map/ppermute | solution.py:246
  111.0 6.2 %copy-start.15 = (s32[160,2]{0,1:T(2,128)S(1)}, s32[160,2]{0,1:T(2,128)}, u32[]{:S(2)}) copy-start(s32[160,2]{0,1:T(2,128)} %param.10) | copy-start | bytes 3844
  111.0 6.3 %copy-start.14 = (f32[160,2]{0,1:T(2,128)S(1)}, f32[160,2]{0,1:T(2,128)}, u32[]{:S(2)}) copy-start(f32[160,2]{0,1:T(2,128)} %param.12) | copy-start | bytes 3844
  111.0 6.5 %copy-start.16 = (f32[160]{0:T(256)S(1)}, f32[160]{0:T(256)}, u32[]{:S(2)}) copy-start(f32[160]{0:T(256)} %param.11) | copy-start | bytes 1924
  111.0 63.5 %copy-start = (bf16[160,2048]{1,0:T(8,128)(2,1)S(1)}, bf16[160,2048]{1,0:T(8,128)(2,1)}, u32[]{:S(2)}) copy-start(bf16[160,2048]{1,0:T(8,128)(2,1)} %tok_ref.3) | copy-start | bytes 1966084
  111.1 63.5 %copy-start.1 = (f32[2048]{0:T(1024)S(1)}, f32[2048]{0:T(1024)}, u32[]{:S(2)}) copy-start(f32[2048]{0:T(1024)} %param.16) | copy-start | bytes 24580
  111.1 63.5 %copy-start.2 = (f32[2048]{0:T(1024)S(1)}, f32[2048]{0:T(1024)}, u32[]{:S(2)}) copy-start(f32[2048]{0:T(1024)} %param.17) | copy-start | bytes 24580
  111.1 63.5 %all-to-all-start.1 = ((bf16[48,40,512]{2,1,0:T(8,128)(2,1)}), bf16[48,40,512]{2,1,0:T(8,128)(2,1)S(1)}, u32[]{:S(2)}, u32[]{:S(2)}) async-start(bf16[48,40,512]{2,1,0:T(8,128)(2,1)} %ffn.1), calls=%async_computation.1 | async-start | bytes 3932160 | tf_op jit(solution)/shard_map/all_to_all | solution.py:266
  (2 other events, 1.5 us)

commit v5 on v4

--- a/solution.py
+++ b/solution.py
@@ -7,7 +7,7 @@
 from jax.experimental.pallas import tpu as pltpu
 from jax.sharding import PartitionSpec as P
 
-TOP = 2
+
 residual_scale = 2.0**0.5
 norm_eps = 1e-05
 BF16 = jnp.bfloat16
@@ -16,7 +16,7 @@
 REST = 2
 QUARTERS = 4
 SLICE = 32
-ROOM = 50 * 2**20
+ROOM = 47 * 2**20
 LATE = 1
 
 
@@ -125,9 +125,10 @@
         copy.wait()
 
 
-def collect_kernel(late_ref, own_ref, *refs):
+def collect_kernel(shared, late_ref, *refs):
     pieces, (out_ref, staged_ref, in_sems, out_sems) = refs[:-4], refs[-4:]
-    half = len(pieces) // 2
+    each = (len(pieces) - shared) // 2
+    count = shared + each
 
     def load(piece, n):
         return pltpu.make_async_copy(piece, staged_ref.at[n], in_sems.at[n])
@@ -135,18 +136,19 @@
     def store(n):
         return pltpu.make_async_copy(staged_ref.at[n], out_ref.at[n], out_sems.at[n])
 
-    load(own_ref, 0).start()
-    for late, chosen in ((0, pieces[:half]), (1, pieces[half:])):
+    for n in range(shared):
+        load(pieces[n], n).start()
+    for late in range(2):
 
         @pl.when(late_ref[0] == late)
         def _():
-            for n, piece in enumerate(chosen):
-                load(piece, n + 1).start()
-
-    for n in range(half + 1):
-        load(own_ref, n).wait()
+            for n in range(each):
+                load(pieces[shared + late * each + n], shared + n).start()
+
+    for n in range(count):
+        load(pieces[0], n).wait()
         store(n).start()
-    for n in range(half + 1):
+    for n in range(count):
         store(n).wait()
 
 
@@ -199,7 +201,11 @@
         return lax.ppermute(x, "tp", [(i, (i + 2 * chips) % size) for i in range(core, size, 2)])
 
     up, down = move(own, 2), move(own, -2)
-    return [up, down, move(own, 1), move(own, -1), move(up, 2), move(up, 1), move(down, -1)]
+    first = [up, down, move(own, 1), move(own, -1)]
+    second = []
+    for x, chips in ((up, 2), (up, 1), (down, -1)):
+        second.append(move(x, chips))
+    return first, second
 
 
 def body(tokens, expert_ids, group_weight, expert_share, gate_w, up_w, down_w, out_gain, out_shift):
@@ -229,22 +235,28 @@
     received = lax.all_to_all(send, "ep", split_axis=0, concat_axis=0, tiled=True)
     own, send = lax.optimization_barrier((own, send))
     early_pieces = ring(own, 1 - LATE)
-    count = len(early_pieces) + 1
-    slices = (count,) + own.shape
-    collected = pl.pallas_call(
-        collect_kernel,
-        out_shape=jax.ShapeDtypeStruct(slices, BF16),
-        in_specs=[smem] + [hbm] * (2 * count - 1),
-        out_specs=hbm,
-        scratch_shapes=[
-            pltpu.VMEM(slices, BF16),
-            pltpu.SemaphoreType.DMA((count,)),
-            pltpu.SemaphoreType.DMA((count,)),
-        ],
-        name="collect",
-    )(late, own, *early_pieces, *late_pieces)
-    other = lax.ppermute(collected, "tp", [(i, i ^ 1) for i in range(lax.axis_size("tp"))])
-    pieces = [p.reshape(count, 3, SLICE, model_width) for p in (collected, other)]
+
+    def collect(shared, first, second):
+        pieces = shared + first + second
+        count = len(shared) + len(first)
+        slices = (count,) + own.shape
+        mine = pl.pallas_call(
+            functools.partial(collect_kernel, len(shared)),
+            out_shape=jax.ShapeDtypeStruct(slices, BF16),
+            in_specs=[smem] + [hbm] * len(pieces),
+            out_specs=hbm,
+            scratch_shapes=[
+                pltpu.VMEM(slices, BF16),
+                pltpu.SemaphoreType.DMA((count,)),
+                pltpu.SemaphoreType.DMA((count,)),
+            ],
+        )(late, *pieces)
+        other = lax.ppermute(mine, "tp", [(i, i ^ 1) for i in range(lax.axis_size("tp"))])
+        return [x.reshape(count, 3, SLICE, model_width) for x in (mine, other)]
+
+    near = collect([own], early_pieces[0], late_pieces[0])
+    far = collect([], early_pieces[1], late_pieces[1])
+    pieces = [near[0], far[0], near[1], far[1]]
     rows = ep_size * (HEAD + REST)
     results = pl.pallas_call(
         functools.partial(ffn_kernel, 2),

time: 178 us -> 195 us (1.096)
  the two profiles are of different devices: /device:TPU:1 before, /device:TPU:16 now
where the time goes in v5:
time: 195 us
  waiting for transfers between devices  93.3 us (48%)
  starting transfers between devices  77.2 us (40%)
  Pallas kernels  17.4 us (9%)
  local copies, waits for them, and re-layouts  5.13 us (3%)
    all_to_all x1, waiting for transfers between devices, body(): lax.all_to_all(results, 'ep', split_axis=0, concat_axis=0, tiled=True)  70.9 us
    ppermute x14, starting transfers between devices, move(): lax.ppermute(x, 'tp', [(i, (i + 2 * chips) % size) for i in range(core, s...  28.1 us
    ppermute x14, waiting for transfers between devices, move(): lax.ppermute(x, 'tp', [(i, (i + 2 * chips) % size) for i in range(core, s...  19.4 us
    ppermute x2, starting transfers between devices, collect(): lax.ppermute(mine, 'tp', [(i, i ^ 1) for i in range(lax.axis_size('tp'))])  18.5 us
    all_to_all x1, starting transfers between devices, body(): lax.all_to_all(send, 'ep', split_axis=0, concat_axis=0, tiled=True)  18.3 us
    all_to_all x1, starting transfers between devices, body(): lax.all_to_all(results, 'ep', split_axis=0, concat_axis=0, tiled=True)  12.3 us
    pallas_call x1, Pallas kernels, body(): pl.pallas_call(functools.partial(ffn_kernel, 2), out_shape=buffer, in_spe...  6.68 us
    unnamed x43, local copies, waits for them, and re-layouts  5.03 us
  transfers between devices with their start and end apart: 18, of which 7 were waited for; matrix products, arithmetic and copies ran while one was open for 0% of the time, Pallas kernels for 4%

profile of v5, /device:TPU:16, one launch (start us, length us, event | category | flops | bytes accessed | tf_op | source)
XLA Modules:
  0.0 194.6 jit_solution(1512492481999668150)
XLA Ops:
  0.0 1.1 pad_maximum_fusion.refs_0_
  1.1 0.7 collective-permute-start
  1.8 0.7 collective-permute-start.1
  3.9 0.7 collective-permute-start.4
  5.3 0.7 collective-permute-start.6
  6.0 3.2 %pack.1._ = bf16[48,40,512]{2,1,0:T(8,128)(2,1)} custom-call(bf16[160,2048]{1,0:T(8,128)(2,1)} %tok_ref.3, s32[2,160]{1,0:T(2,128)} %bitcast.19), custom_call_target="tpu_custom_call" | custom-call | tf_op jit(solution)/shard_map/pack/pallas_call | solution.py:223
  9.3 0.7 copy-done.8
  10.5 18.3 %all-to-all-start = ((bf16[48,40,512]{2,1,0:T(8,128)(2,1)}), bf16[48,40,512]{2,1,0:T(8,128)(2,1)S(1)}, u32[]{:S(2)}, u32[]{:S(2)}) async-start(bf16[48,40,512]{2,1,0:T(8,128)(2,1)} %pack.1._), calls=%async_computation | async-start | bytes 3932160 | tf_op jit(solution)/shard_map/all_to_all | solution.py:235
  28.8 5.7 %collective-permute-start.7 = (bf16[96,2048]{1,0:T(8,128)(2,1)S(1)}, bf16[96,2048]{1,0:T(8,128)(2,1)S(1)}, u32[]{:S(2)}, u32[]{:S(2)}) collective-permute-start(bf16[96,2048]{1,0:T(8,128)(2,1)S(1)} %pad_maximum_fusion.refs_0_), channel_id=1, source_target_pairs={{0,4},{2,6},{4,8},{6,10},{8,12},{10,14},{12,0},{14,2},{16,20},{18,... | collective-permute-start | bytes 1179656 | tf_op jit(solution)/shard_map/ppermute | solution.py:201
  34.5 1.9 collective-permute-start.8
  36.5 2.7 %collective-permute-start.10 = (bf16[96,2048]{1,0:T(8,128)(2,1)S(1)}, bf16[96,2048]{1,0:T(8,128)(2,1)S(1)}, u32[]{:S(2)}, u32[]{:S(2)}) collective-permute-start(bf16[96,2048]{1,0:T(8,128)(2,1)S(1)} %pad_maximum_fusion.refs_0_), channel_id=1, source_target_pairs={{0,14},{2,0},{4,2},{6,4},{8,6},{10,8},{12,10},{14,12},{16,30},{18,... | collective-permute-start | bytes 1179656 | tf_op jit(solution)/shard_map/ppermute | solution.py:201
  39.2 3.2 %collective-permute-start.9 = (bf16[96,2048]{1,0:T(8,128)(2,1)S(1)}, bf16[96,2048]{1,0:T(8,128)(2,1)}, u32[]{:S(2)}, u32[]{:S(2)}) collective-permute-start(bf16[96,2048]{1,0:T(8,128)(2,1)S(1)} %pad_maximum_fusion.refs_0_), channel_id=1, source_target_pairs={{0,2},{2,4},{4,6},{6,8},{8,10},{10,12},{12,14},{14,0},{16,18},{18,... | collective-permute-start | bytes 1179656 | tf_op jit(solution)/shard_map/ppermute | solution.py:201
  42.4 1.6 collective-permute-done.7.refs_1_
  44.0 6.7 %collective-permute-done.8.refs_2_ = bf16[96,2048]{1,0:T(8,128)(2,1)S(1)} collective-permute-done((bf16[96,2048]{1,0:T(8,128)(2,1)S(1)}, bf16[96,2048]{1,0:T(8,128)(2,1)S(1)}, u32[]{:S(2)}, u32[]{:S(2)}) %collective-permute-start.8) | collective-permute-done | bytes 393248 | tf_op jit(solution)/shard_map/ppermute | solution.py:201
  50.7 0.7 collective-permute-done.10.refs_4_
  52.1 2.3 %shard_map.91 = bf16[5,96,2048]{2,1,0:T(8,128)(2,1)} custom-call(s32[1]{0:T(128)} %bitcast.4.late_ref, bf16[96,2048]{1,0:T(8,128)(2,1)} %copy-done.4, bf16[96,2048]{1,0:T(8,128)(2,1)} %copy-done.9, bf16[96,2048]{1,0:T(8,128)(2,1)} %copy-done.10, bf16[96,2048]{1,0:T(8,128)(2,1)} %collective-permute-done.9.refs_3_, bf16[96,2048]{1,0:T(8,128)(2,1)} %copy-done.11, ...), custom_call_target="tpu_custom_call" | custom-call | tf_op jit(solution)/shard_map/pallas_call | solution.py:243
  54.5 16.6 %collective-permute-start.14 = (bf16[5,96,2048]{2,1,0:T(8,128)(2,1)}, bf16[5,96,2048]{2,1,0:T(8,128)(2,1)}, u32[]{:S(2)}, u32[]{:S(2)}) collective-permute-start(bf16[5,96,2048]{2,1,0:T(8,128)(2,1)} %shard_map.91), channel_id=1, source_target_pairs={{0,1},{1,0},{2,3},{3,2},{4,5},{5,4},{6,7},{7,6},{8,9},{9,8},{10,11... | collective-permute-start | bytes 5898248 | tf_op jit(solution)/shard_map/ppermute | solution.py:254
  71.0 4.0 %collective-permute-start.11 = (bf16[96,2048]{1,0:T(8,128)(2,1)}, bf16[96,2048]{1,0:T(8,128)(2,1)S(1)}, u32[]{:S(2)}, u32[]{:S(2)}) collective-permute-start(bf16[96,2048]{1,0:T(8,128)(2,1)} %copy-done.9), channel_id=1, source_target_pairs={{0,4},{2,6},{4,8},{6,10},{8,12},{10,14},{12,0},{14,2},{16,20},{18,... | collective-permute-start | bytes 1179656 | tf_op jit(solution)/shard_map/ppermute | solution.py:201
  75.1 3.0 %collective-permute-start.12 = (bf16[96,2048]{1,0:T(8,128)(2,1)}, bf16[96,2048]{1,0:T(8,128)(2,1)S(1)}, u32[]{:S(2)}, u32[]{:S(2)}) collective-permute-start(bf16[96,2048]{1,0:T(8,128)(2,1)} %copy-done.9), channel_id=1, source_target_pairs={{0,2},{2,4},{4,6},{6,8},{8,10},{10,12},{12,14},{14,0},{16,18},{18,... | collective-permute-start | bytes 1179656 | tf_op jit(solution)/shard_map/ppermute | solution.py:201
  78.1 2.8 %collective-permute-start.13 = (bf16[96,2048]{1,0:T(8,128)(2,1)}, bf16[96,2048]{1,0:T(8,128)(2,1)S(1)}, u32[]{:S(2)}, u32[]{:S(2)}) collective-permute-start(bf16[96,2048]{1,0:T(8,128)(2,1)} %copy-done.10), channel_id=1, source_target_pairs={{0,14},{2,0},{4,2},{6,4},{8,6},{10,8},{12,10},{14,12},{16,30},{18,... | collective-permute-start | bytes 1179656 | tf_op jit(solution)/shard_map/ppermute | solution.py:201
  80.9 5.0 %collective-permute-done.11.refs_0_ = bf16[96,2048]{1,0:T(8,128)(2,1)S(1)} collective-permute-done((bf16[96,2048]{1,0:T(8,128)(2,1)}, bf16[96,2048]{1,0:T(8,128)(2,1)S(1)}, u32[]{:S(2)}, u32[]{:S(2)}) %collective-permute-start.11) | collective-permute-done | bytes 393248 | tf_op jit(solution)/shard_map/ppermute | solution.py:201
  85.9 5.4 %collective-permute-done.12.refs_1_ = bf16[96,2048]{1,0:T(8,128)(2,1)S(1)} collective-permute-done((bf16[96,2048]{1,0:T(8,128)(2,1)}, bf16[96,2048]{1,0:T(8,128)(2,1)S(1)}, u32[]{:S(2)}, u32[]{:S(2)}) %collective-permute-start.12) | collective-permute-done | bytes 393248 | tf_op jit(solution)/shard_map/ppermute | solution.py:201
  91.3 0.8 copy-done.16
  92.1 0.8 copy-done.17
  92.9 2.1 %shard_map.92 = bf16[3,96,2048]{2,1,0:T(8,128)(2,1)} custom-call(s32[1]{0:T(128)} %bitcast.4.late_ref, bf16[96,2048]{1,0:T(8,128)(2,1)} %copy-done.15, bf16[96,2048]{1,0:T(8,128)(2,1)} %copy-done.16, bf16[96,2048]{1,0:T(8,128)(2,1)} %copy-done.17, bf16[96,2048]{1,0:T(8,128)(2,1)} %copy-done.12, bf16[96,2048]{1,0:T(8,128)(2,1)} %copy-done.13, ...), custom_call_target="tpu_custom_call" | custom-call | tf_op jit(solution)/shard_map/pallas_call | solution.py:243
  95.0 1.9 collective-permute-start.15
  96.9 3.0 %collective-permute-done.15 = bf16[3,96,2048]{2,1,0:T(8,128)(2,1)S(1)} collective-permute-done((bf16[3,96,2048]{2,1,0:T(8,128)(2,1)}, bf16[3,96,2048]{2,1,0:T(8,128)(2,1)S(1)}, u32[]{:S(2)}, u32[]{:S(2)}) %collective-permute-start.15) | collective-permute-done | bytes 1179680 | tf_op jit(solution)/shard_map/ppermute | solution.py:254
  99.9 1.3 copy-done
  101.2 6.7 %ffn.1 = bf16[48,40,512]{2,1,0:T(8,128)(2,1)} custom-call(bf16[48,40,512]{2,1,0:T(8,128)(2,1)S(1)} %all-to-all-done.recv_ref, bf16[48,40,512]{2,1,0:T(8,128)(2,1)} %pack.1._, bf16[5,3,32,2048]{3,2,1,0:T(8,128)(2,1)} %bitcast.15, bf16[3,3,32,2048]{3,2,1,0:T(8,128)(2,1)S(1)} %bitcast.11, ...), custom_call_target="tpu_custom_call", output_to_operand_aliasing={{}: (1, {})} | custom-call | tf_op jit(solution)/shard_map/ffn/pallas_call | solution.py:261
  108.0 12.3 %all-to-all-start.1 = ((bf16[48,40,512]{2,1,0:T(8,128)(2,1)}), bf16[48,40,512]{2,1,0:T(8,128)(2,1)S(1)}, u32[]{:S(2)}, u32[]{:S(2)}) async-start(bf16[48,40,512]{2,1,0:T(8,128)(2,1)} %ffn.1), calls=%async_computation.1 | async-start | bytes 3932160 | tf_op jit(solution)/shard_map/all_to_all | solution.py:278
  120.6 70.9 %all-to-all-done.1.back_ref = bf16[48,40,512]{2,1,0:T(8,128)(2,1)S(1)} async-done(((bf16[48,40,512]{2,1,0:T(8,128)(2,1)}), bf16[48,40,512]{2,1,0:T(8,128)(2,1)S(1)}, u32[]{:S(2)}, u32[]{:S(2)}) %all-to-all-start.1) | async-done | bytes 1966112 | tf_op jit(solution)/shard_map/all_to_all | solution.py:278
  191.5 3.1 %mix.1 = bf16[160,2048]{1,0:T(8,128)(2,1)} custom-call(bf16[48,40,512]{2,1,0:T(8,128)(2,1)S(1)} %all-to-all-done.1.back_ref, bf16[160,2048]{1,0:T(8,128)(2,1)S(1)} %copy-done.1, s32[160,2]{1,0:T(8,128)S(1)} %copy.16.ids_ref, f32[160,2]{1,0:T(8,128)S(1)} %broadcast_multiply_fusion.weight_ref, f32[1,2048]{1,0:T(1,128)S(1)} %bitcast.13, f32[1,2048]{1,0:T(1,128)S(1)} %bitcast.14), custom_call_target="tpu_custom_call" | custom-call | tf_op jit(solution)/shard_map/mix/pallas_call | solution.py:281
  (57 shorter events, 3.8 us)
Async XLA Ops:
  1.1 38.1 %copy-start.4 = (bf16[96,2048]{1,0:T(8,128)(2,1)}, bf16[96,2048]{1,0:T(8,128)(2,1)S(1)}, u32[]{:S(2)}) copy-start(bf16[96,2048]{1,0:T(8,128)(2,1)S(1)} %pad_maximum_fusion.refs_0_) | copy-start | bytes 1179652
  1.1 2.8 %collective-permute-start = (bf16[96,2048]{1,0:T(8,128)(2,1)S(1)}, bf16[96,2048]{1,0:T(8,128)(2,1)S(1)}, u32[]{:S(2)}, u32[]{:S(2)}) collective-permute-start(bf16[96,2048]{1,0:T(8,128)(2,1)S(1)} %pad_maximum_fusion.refs_0_), channel_id=1, source_target_pairs={{1,5},{3,7},{5,9},{7,11},{9,13},{11,15},{13,1},{15,3},{17,21},{19,... | collective-permute-start | bytes 1179656 | tf_op jit(solution)/shard_map/ppermute | solution.py:201
  1.8 3.5 %collective-permute-start.1 = (bf16[96,2048]{1,0:T(8,128)(2,1)S(1)}, bf16[96,2048]{1,0:T(8,128)(2,1)S(1)}, u32[]{:S(2)}, u32[]{:S(2)}) collective-permute-start(bf16[96,2048]{1,0:T(8,128)(2,1)S(1)} %pad_maximum_fusion.refs_0_), channel_id=1, source_target_pairs={{1,13},{3,15},{5,1},{7,3},{9,5},{11,7},{13,9},{15,11},{17,29},{19,... | collective-permute-start | bytes 1179656 | tf_op jit(solution)/shard_map/ppermute | solution.py:201
  2.5 6.7 %collective-permute-start.2 = (bf16[96,2048]{1,0:T(8,128)(2,1)S(1)}, bf16[96,2048]{1,0:T(8,128)(2,1)S(1)}, u32[]{:S(2)}, u32[]{:S(2)}) collective-permute-start(bf16[96,2048]{1,0:T(8,128)(2,1)S(1)} %pad_maximum_fusion.refs_0_), channel_id=1, source_target_pairs={{1,3},{3,5},{5,7},{7,9},{9,11},{11,13},{13,15},{15,1},{17,19},{19,... | collective-permute-start | bytes 1179656 | tf_op jit(solution)/shard_map/ppermute | solution.py:201
  3.2 6.0 %collective-permute-start.3 = (bf16[96,2048]{1,0:T(8,128)(2,1)S(1)}, bf16[96,2048]{1,0:T(8,128)(2,1)S(1)}, u32[]{:S(2)}, u32[]{:S(2)}) collective-permute-start(bf16[96,2048]{1,0:T(8,128)(2,1)S(1)} %pad_maximum_fusion.refs_0_), channel_id=1, source_target_pairs={{1,15},{3,1},{5,3},{7,5},{9,7},{11,9},{13,11},{15,13},{17,31},{19,... | collective-permute-start | bytes 1179656 | tf_op jit(solution)/shard_map/ppermute | solution.py:201
  3.9 6.6 %copy-start.5 = (bf16[96,2048]{1,0:T(8,128)(2,1)}, bf16[96,2048]{1,0:T(8,128)(2,1)S(1)}, u32[]{:S(2)}) copy-start(bf16[96,2048]{1,0:T(8,128)(2,1)S(1)} %collective-permute-done.refs_5_) | copy-start | bytes 1179652
  3.9 5.3 %collective-permute-start.4 = (bf16[96,2048]{1,0:T(8,128)(2,1)S(1)}, bf16[96,2048]{1,0:T(8,128)(2,1)S(1)}, u32[]{:S(2)}, u32[]{:S(2)}) collective-permute-start(bf16[96,2048]{1,0:T(8,128)(2,1)S(1)} %collective-permute-done.refs_5_), channel_id=1, source_target_pairs={{1,5},{3,7},{5,9},{7,11},{9,13},{11,15},{13,1},{15,3},{17,21},{19,... | collective-permute-start | bytes 1179656 | tf_op jit(solution)/shard_map/ppermute | solution.py:201
  4.6 4.7 %collective-permute-start.5 = (bf16[96,2048]{1,0:T(8,128)(2,1)S(1)}, bf16[96,2048]{1,0:T(8,128)(2,1)S(1)}, u32[]{:S(2)}, u32[]{:S(2)}) collective-permute-start(bf16[96,2048]{1,0:T(8,128)(2,1)S(1)} %collective-permute-done.refs_5_), channel_id=1, source_target_pairs={{1,3},{3,5},{5,7},{7,9},{9,11},{11,13},{13,15},{15,1},{17,19},{19,... | collective-permute-start | bytes 1179656 | tf_op jit(solution)/shard_map/ppermute | solution.py:201
  5.3 5.2 %copy-start.6 = (bf16[96,2048]{1,0:T(8,128)(2,1)}, bf16[96,2048]{1,0:T(8,128)(2,1)S(1)}, u32[]{:S(2)}) copy-start(bf16[96,2048]{1,0:T(8,128)(2,1)S(1)} %collective-permute-done.1.refs_6_) | copy-start | bytes 1179652
  5.3 4.0 %collective-permute-start.6 = (bf16[96,2048]{1,0:T(8,128)(2,1)S(1)}, bf16[96,2048]{1,0:T(8,128)(2,1)S(1)}, u32[]{:S(2)}, u32[]{:S(2)}) collective-permute-start(bf16[96,2048]{1,0:T(8,128)(2,1)S(1)} %collective-permute-done.1.refs_6_), channel_id=1, source_target_pairs={{1,15},{3,1},{5,3},{7,5},{9,7},{11,9},{13,11},{15,13},{17,31},{19,... | collective-permute-start | bytes 1179656 | tf_op jit(solution)/shard_map/ppermute | solution.py:201
  9.2 1.4 copy-start.7
  9.3 1.2 copy-start.14
  10.5 89.4 %all-to-all-start = ((bf16[48,40,512]{2,1,0:T(8,128)(2,1)}), bf16[48,40,512]{2,1,0:T(8,128)(2,1)S(1)}, u32[]{:S(2)}, u32[]{:S(2)}) async-start(bf16[48,40,512]{2,1,0:T(8,128)(2,1)} %pack.1._), calls=%async_computation | async-start | bytes 3932160 | tf_op jit(solution)/shard_map/all_to_all | solution.py:235
  28.8 15.1 %collective-permute-start.7 = (bf16[96,2048]{1,0:T(8,128)(2,1)S(1)}, bf16[96,2048]{1,0:T(8,128)(2,1)S(1)}, u32[]{:S(2)}, u32[]{:S(2)}) collective-permute-start(bf16[96,2048]{1,0:T(8,128)(2,1)S(1)} %pad_maximum_fusion.refs_0_), channel_id=1, source_target_pairs={{0,4},{2,6},{4,8},{6,10},{8,12},{10,14},{12,0},{14,2},{16,20},{18,... | collective-permute-start | bytes 1179656 | tf_op jit(solution)/shard_map/ppermute | solution.py:201
  34.5 16.1 %collective-permute-start.8 = (bf16[96,2048]{1,0:T(8,128)(2,1)S(1)}, bf16[96,2048]{1,0:T(8,128)(2,1)S(1)}, u32[]{:S(2)}, u32[]{:S(2)}) collective-permute-start(bf16[96,2048]{1,0:T(8,128)(2,1)S(1)} %pad_maximum_fusion.refs_0_), channel_id=1, source_target_pairs={{0,12},{2,14},{4,0},{6,2},{8,4},{10,6},{12,8},{14,10},{16,28},{18,... | collective-permute-start | bytes 1179656 | tf_op jit(solution)/shard_map/ppermute | solution.py:201
  36.5 14.9 %collective-permute-start.10 = (bf16[96,2048]{1,0:T(8,128)(2,1)S(1)}, bf16[96,2048]{1,0:T(8,128)(2,1)S(1)}, u32[]{:S(2)}, u32[]{:S(2)}) collective-permute-start(bf16[96,2048]{1,0:T(8,128)(2,1)S(1)} %pad_maximum_fusion.refs_0_), channel_id=1, source_target_pairs={{0,14},{2,0},{4,2},{6,4},{8,6},{10,8},{12,10},{14,12},{16,30},{18,... | collective-permute-start | bytes 1179656 | tf_op jit(solution)/shard_map/ppermute | solution.py:201
  39.2 12.2 %collective-permute-start.9 = (bf16[96,2048]{1,0:T(8,128)(2,1)S(1)}, bf16[96,2048]{1,0:T(8,128)(2,1)}, u32[]{:S(2)}, u32[]{:S(2)}) collective-permute-start(bf16[96,2048]{1,0:T(8,128)(2,1)S(1)} %pad_maximum_fusion.refs_0_), channel_id=1, source_target_pairs={{0,2},{2,4},{4,6},{6,8},{8,10},{10,12},{12,14},{14,0},{16,18},{18,... | collective-permute-start | bytes 1179656 | tf_op jit(solution)/shard_map/ppermute | solution.py:201
  44.0 7.4 %copy-start.9 = (bf16[96,2048]{1,0:T(8,128)(2,1)}, bf16[96,2048]{1,0:T(8,128)(2,1)S(1)}, u32[]{:S(2)}) copy-start(bf16[96,2048]{1,0:T(8,128)(2,1)S(1)} %collective-permute-done.7.refs_1_) | copy-start | bytes 1179652
  54.5 45.4 %collective-permute-start.14 = (bf16[5,96,2048]{2,1,0:T(8,128)(2,1)}, bf16[5,96,2048]{2,1,0:T(8,128)(2,1)}, u32[]{:S(2)}, u32[]{:S(2)}) collective-permute-start(bf16[5,96,2048]{2,1,0:T(8,128)(2,1)} %shard_map.91), channel_id=1, source_target_pairs={{0,1},{1,0},{2,3},{3,2},{4,5},{5,4},{6,7},{7,6},{8,9},{9,8},{10,11... | collective-permute-start | bytes 5898248 | tf_op jit(solution)/shard_map/ppermute | solution.py:254
  71.0 14.9 %collective-permute-start.11 = (bf16[96,2048]{1,0:T(8,128)(2,1)}, bf16[96,2048]{1,0:T(8,128)(2,1)S(1)}, u32[]{:S(2)}, u32[]{:S(2)}) collective-permute-start(bf16[96,2048]{1,0:T(8,128)(2,1)} %copy-done.9), channel_id=1, source_target_pairs={{0,4},{2,6},{4,8},{6,10},{8,12},{10,14},{12,0},{14,2},{16,20},{18,... | collective-permute-start | bytes 1179656 | tf_op jit(solution)/shard_map/ppermute | solution.py:201
  75.1 16.2 %collective-permute-start.12 = (bf16[96,2048]{1,0:T(8,128)(2,1)}, bf16[96,2048]{1,0:T(8,128)(2,1)S(1)}, u32[]{:S(2)}, u32[]{:S(2)}) collective-permute-start(bf16[96,2048]{1,0:T(8,128)(2,1)} %copy-done.9), channel_id=1, source_target_pairs={{0,2},{2,4},{4,6},{6,8},{8,10},{10,12},{12,14},{14,0},{16,18},{18,... | collective-permute-start | bytes 1179656 | tf_op jit(solution)/shard_map/ppermute | solution.py:201
  78.1 13.2 %collective-permute-start.13 = (bf16[96,2048]{1,0:T(8,128)(2,1)}, bf16[96,2048]{1,0:T(8,128)(2,1)S(1)}, u32[]{:S(2)}, u32[]{:S(2)}) collective-permute-start(bf16[96,2048]{1,0:T(8,128)(2,1)} %copy-done.10), channel_id=1, source_target_pairs={{0,14},{2,0},{4,2},{6,4},{8,6},{10,8},{12,10},{14,12},{16,30},{18,... | collective-permute-start | bytes 1179656 | tf_op jit(solution)/shard_map/ppermute | solution.py:201
  85.9 5.4 %copy-start.15 = (bf16[96,2048]{1,0:T(8,128)(2,1)}, bf16[96,2048]{1,0:T(8,128)(2,1)S(1)}, u32[]{:S(2)}) copy-start(bf16[96,2048]{1,0:T(8,128)(2,1)S(1)} %collective-permute-done.11.refs_0_) | copy-start | bytes 1179652
  95.0 5.0 %collective-permute-start.15 = (bf16[3,96,2048]{2,1,0:T(8,128)(2,1)}, bf16[3,96,2048]{2,1,0:T(8,128)(2,1)S(1)}, u32[]{:S(2)}, u32[]{:S(2)}) collective-permute-start(bf16[3,96,2048]{2,1,0:T(8,128)(2,1)} %shard_map.92), channel_id=1, source_target_pairs={{0,1},{1,0},{2,3},{3,2},{4,5},{5,4},{6,7},{7,6},{8,9},{9,8},{10,11... | collective-permute-start | bytes 3538952 | tf_op jit(solution)/shard_map/ppermute | solution.py:254
  99.9 1.3 copy-start
  107.9 12.4 %copy-start.19 = (s32[160,2]{0,1:T(2,128)S(1)}, s32[160,2]{0,1:T(2,128)}, u32[]{:S(2)}) copy-start(s32[160,2]{0,1:T(2,128)} %param.10) | copy-start | bytes 3844
  107.9 12.5 %copy-start.18 = (f32[160,2]{0,1:T(2,128)S(1)}, f32[160,2]{0,1:T(2,128)}, u32[]{:S(2)}) copy-start(f32[160,2]{0,1:T(2,128)} %param.12) | copy-start | bytes 3844
  107.9 12.6 %copy-start.20 = (f32[160]{0:T(256)S(1)}, f32[160]{0:T(256)}, u32[]{:S(2)}) copy-start(f32[160]{0:T(256)} %param.11) | copy-start | bytes 1924
  107.9 83.6 %copy-start.1 = (bf16[160,2048]{1,0:T(8,128)(2,1)S(1)}, bf16[160,2048]{1,0:T(8,128)(2,1)}, u32[]{:S(2)}) copy-start(bf16[160,2048]{1,0:T(8,128)(2,1)} %tok_ref.3) | copy-start | bytes 1966084
  107.9 83.6 %copy-start.2 = (f32[2048]{0:T(1024)S(1)}, f32[2048]{0:T(1024)}, u32[]{:S(2)}) copy-start(f32[2048]{0:T(1024)} %param.16) | copy-start | bytes 24580
  107.9 83.6 %copy-start.3 = (f32[2048]{0:T(1024)S(1)}, f32[2048]{0:T(1024)}, u32[]{:S(2)}) copy-start(f32[2048]{0:T(1024)} %param.17) | copy-start | bytes 24580
  108.0 83.5 %all-to-all-start.1 = ((bf16[48,40,512]{2,1,0:T(8,128)(2,1)}), bf16[48,40,512]{2,1,0:T(8,128)(2,1)S(1)}, u32[]{:S(2)}, u32[]{:S(2)}) async-start(bf16[48,40,512]{2,1,0:T(8,128)(2,1)} %ffn.1), calls=%async_computation.1 | async-start | bytes 3932160 | tf_op jit(solution)/shard_map/all_to_all | solution.py:278
  (7 other events, 5.8 us)

commit v6 on v3

--- a/solution.py
+++ b/solution.py
@@ -17,6 +17,8 @@
 QUARTERS = 4
 SLICE = 32
 ROOM = 50 * 2**20
+LATE = 1
+HOLD = 27000
 
 
 def dot(a, b):
@@ -71,17 +73,19 @@
 
 
 def ffn_kernel(
-    chunks, recv_ref, gathered_ref, _, out_ref, weight_ref, rows_ref, hidden_ref, staged_ref, sems, out_sems
+    chunks, recv_ref, _, *refs
 ):
+    pieces, (out_ref, weight_ref, rows_ref, hidden_ref, staged_ref, sems, out_sems) = refs[:-7], refs[-7:]
     sources, _, width = recv_ref.shape
     heads, rests = sources * HEAD, sources * REST
     slices, _, _, model_width = weight_ref.shape
     size = slices // chunks
     waits = []
-    for i in range(chunks):
-        part = pl.ds(i * size, size)
-        waits.append(pltpu.make_async_copy(gathered_ref.at[part], weight_ref.at[part], sems.at[i]))
-        waits[i].start()
+    for n in range(chunks):
+        part = pl.ds(n * size, size)
+        copy = pltpu.make_async_copy(pieces[0].at[part], weight_ref.at[part], sems.at[n])
+        copy.start()
+        waits.append(((n + 1) * size, copy))
 
     def pick(q):
         a = iota((rests, heads), 0)
@@ -98,7 +102,9 @@
         rows_ref[heads:, cols] = dot(pick(q), rest).astype(BF16)
 
     for i in range(chunks):
-        waits[i].wait()
+        for end, copy in waits:
+            if i * size < end <= (i + 1) * size:
+                copy.wait()
         part = slice(i * size, (i + 1) * size)
         gate = dot_nt(rows_ref[...], weight_ref[part, 0].reshape(-1, model_width))
         up = dot_nt(rows_ref[...], weight_ref[part, 1].reshape(-1, model_width))
@@ -118,6 +124,12 @@
     sent.append(send_out(staged_ref, out_ref, out_sems, QUARTERS))
     for copy in sent:
         copy.wait()
+
+
+def hold_kernel(nanos_ref, _, out_ref):
+    @pl.when(nanos_ref[0] > 0)
+    def _():
+        pl.delay(nanos_ref[0])
 
 
 def mix_kernel(back_ref, tok_ref, ids_ref, weight_ref, gain_ref, shift_ref, out_ref, sum_ref):
@@ -160,23 +172,6 @@
     center = sum_ref[...] - total / model_width
     variance = jnp.mean(center * center, axis=-1, keepdims=True)
     out_ref[...] = (center * lax.rsqrt(variance + norm_eps) * gain_ref[...] + shift_ref[...]).astype(BF16)
-
-
-def gather_slices(own):
-    size = lax.axis_size("tp")
-    partner = [(i, i ^ 1) for i in range(size)]
-    onward = [(i, (i + 2 - 4 * (i % 2)) % size) for i in range(size)]
-    other = lax.ppermute(own, "tp", partner)
-    pieces = [own, other]
-    chains = [own, other]
-    steps = size // 4
-    for step in range(steps):
-        if step == steps - 1:
-            chains = chains[:1]
-        chains = [lax.ppermute(c, "tp", onward) for c in chains]
-        pieces += chains
-        pieces += [lax.ppermute(c, "tp", partner) for c in chains]
-    return jnp.concatenate(pieces, axis=0)
 
 
 def body(tokens, expert_ids, group_weight, expert_share, gate_w, up_w, down_w, out_gain, out_shift):
@@ -198,27 +193,38 @@
         scratch_shapes=[staged, staged_sems],
         name="pack",
     )(tokens, expert_ids.T)
+    own = jnp.concatenate([gate_w[0], up_w[0], down_w[0]], axis=0)
+    gathered = lax.all_gather(own, "tp", axis=0, tiled=True)
+    late = (lax.axis_index("tp") % 2 == LATE).astype(jnp.int32).reshape(1)
+    send = pl.pallas_call(
+        hold_kernel,
+        out_shape=buffer,
+        in_specs=[pl.BlockSpec(memory_space=pltpu.SMEM), hbm],
+        out_specs=hbm,
+        input_output_aliases={1: 0},
+        compiler_params=pltpu.CompilerParams(has_side_effects=True),
+        name="hold",
+    )(late * HOLD, send)
     received = lax.all_to_all(send, "ep", split_axis=0, concat_axis=0, tiled=True)
-    own = jnp.concatenate([gate_w[0], up_w[0], down_w[0]], axis=0)
-    gathered = gather_slices(own).reshape(-1, 3, SLICE, model_width)
+    pieces = [gathered.reshape(-1, 3, SLICE, model_width)]
     rows = ep_size * (HEAD + REST)
     results = pl.pallas_call(
         functools.partial(ffn_kernel, 2),
         out_shape=buffer,
-        in_specs=[vmem, hbm, hbm],
+        in_specs=[vmem] + [hbm] * (len(pieces) + 1),
         out_specs=hbm,
         scratch_shapes=[
-            pltpu.VMEM(gathered.shape, BF16),
+            pltpu.VMEM((hidden // SLICE, 3, SLICE, model_width), BF16),
             pltpu.VMEM((rows, model_width), BF16),
             pltpu.VMEM((rows, hidden), BF16),
             staged,
             pltpu.SemaphoreType.DMA((2,)),
             staged_sems,
         ],
-        input_output_aliases={2: 0},
+        input_output_aliases={1: 0},
         compiler_params=pltpu.CompilerParams(vmem_limit_bytes=ROOM),
         name="ffn",
-    )(received, gathered, send)
+    )(received, send, *pieces)
     back = lax.all_to_all(results, "ep", split_axis=0, concat_axis=0, tiled=True)
     share_norm = expert_share / jnp.sum(expert_share, axis=1, keepdims=True)
     route_weight = group_weight[:, None] * share_norm

time: 184 us -> 178 us (0.967); the launches traced: 182 us -> 178 us
  blocking collectives: 0 us -> 92.8 us
  starting transfers between devices: 78.2 us -> 5.1 us
  waiting for transfers between devices: 75.8 us -> 50.8 us
  local copies, waits for them, and re-layouts: 14 us -> 0.25 us
  between operations: 0.32 us -> 13.5 us
    all_to_all x0 -> x1, blocking collectives: none -> 92.8 us  [body(): lax.all_to_all(send, 'ep', split_axis=0, concat_axis=0, tiled=True)]
    ppermute x15 -> x0, starting transfers between devices: 47.7 us -> none  [the longest x7 24.7 us: gather_slices(): chains = [lax.ppermute(c, 'tp', onward) for c in chains]]
    all_to_all x1 -> x0, starting transfers between devices: 18.8 us -> none  [body(): lax.all_to_all(send, 'ep', split_axis=0, concat_axis=0, tiled=True)]
    all_to_all x1, waiting for transfers between devices: 69.6 us -> 50.8 us  [body(): lax.all_to_all(results, 'ep', split_axis=0, concat_axis=0, tiled=True)]
    unnamed x36 -> x13, local copies, waits for them, and re-layouts: 13.1 us -> 0.15 us
    all_to_all x1, starting transfers between devices: 11.7 us -> 5.1 us  [body(): lax.all_to_all(results, 'ep', split_axis=0, concat_axis=0, tiled=True)]
    ppermute x15 -> x0, waiting for transfers between devices: 5.8 us -> none  [the longest x7 5.78 us: gather_slices(): chains = [lax.ppermute(c, 'tp', onward) for c in chains]]
  transfers between devices with their start and end apart: 17 -> 2, of which waited for: 5 -> 1; matrix products, arithmetic and copies ran while one was open for 8% -> 0% of each run, Pallas kernels for 0% -> 2%
where the time goes in v6:
time: 178 us
  blocking collectives  92.8 us (52%)
  waiting for transfers between devices  50.8 us (29%)
  Pallas kernels  13.7 us (8%)
  between operations  13.5 us (8%)
  starting transfers between devices  5.1 us (3%)
  other arithmetic  1.91 us (1%)
    all_to_all x1, blocking collectives, body(): lax.all_to_all(send, 'ep', split_axis=0, concat_axis=0, tiled=True)  92.8 us
    all_to_all x1, waiting for transfers between devices, body(): lax.all_to_all(results, 'ep', split_axis=0, concat_axis=0, tiled=True)  50.8 us
    pallas_call x1, Pallas kernels, body(): pl.pallas_call(functools.partial(ffn_kernel, 2), out_shape=buffer, in_spe...  7.35 us
    all_to_all x1, starting transfers between devices, body(): lax.all_to_all(results, 'ep', split_axis=0, concat_axis=0, tiled=True)  5.1 us
  transfers between devices with their start and end apart: 2, of which 1 were waited for; matrix products, arithmetic and copies ran while one was open for 0% of the time, Pallas kernels for 2%

profile of v6, /device:TPU:1, one launch (start us, length us, event | category | flops | bytes accessed | tf_op | source)
XLA Modules:
  0.0 178.2 jit_solution(2854732679693659348)
XLA Ops:
  6.5 0.0 all-gather.2.cloned.1.call-start
  6.5 1.8 %pad_maximum_fusion = bf16[96,2048]{1,0:T(8,128)(2,1)} fusion(bf16[32,2048]{1,0:T(8,128)(2,1)} %bitcast.11, bf16[32,2048]{1,0:T(8,128)(2,1)} %bitcast.12, bf16[32,2048]{1,0:T(8,128)(2,1)} %bitcast.13), kind=kLoop, calls=%fused_computation | loop fusion | flops 1179648 | bytes 786432 | tf_op jit(solution)/shard_map/concatenate | solution.py:196
  8.3 0.0 all-gather.2.cloned.1.call-update
  8.4 3.2 %pack.1._ = bf16[48,40,512]{2,1,0:T(8,128)(2,1)} custom-call(bf16[160,2048]{1,0:T(8,128)(2,1)} %tok_ref.3, s32[2,160]{1,0:T(2,128)} %bitcast.14), custom_call_target="tpu_custom_call" | custom-call | tf_op jit(solution)/shard_map/pack/pallas_call | solution.py:189
  11.7 92.8 %all_to_all.10.recv_ref = bf16[48,40,512]{2,1,0:T(8,128)(2,1)S(1)} all-to-all(bf16[48,40,512]{2,1,0:T(8,128)(2,1)} %hold.1._), channel_id=1, replica_groups=mesh['ep'=48,'tp'=16] {'ep'}, dimensions={0} | all-to-all | bytes 3932160 | tf_op jit(solution)/shard_map/all_to_all | solution.py:208
  104.5 0.0 all-gather.2.cloned.1.call-done
  104.5 7.4 %ffn.1 = bf16[48,40,512]{2,1,0:T(8,128)(2,1)} custom-call(bf16[48,40,512]{2,1,0:T(8,128)(2,1)S(1)} %all_to_all.10.recv_ref, bf16[48,40,512]{2,1,0:T(8,128)(2,1)} %hold.1._, bf16[16,3,32,2048]{3,2,1,0:T(8,128)(2,1)} %bitcast.10), custom_call_target="tpu_custom_call", output_to_operand_aliasing={{}: (1, {})} | custom-call | tf_op jit(solution)/shard_map/ffn/pallas_call | solution.py:211
  111.8 0.0 copy-start.4
  111.9 0.0 copy-start.3
  111.9 0.0 copy-start.5
  111.9 0.0 copy-start
  111.9 0.0 copy-start.1
  111.9 0.0 copy-start.2
  111.9 5.1 %all-to-all-start.1 = ((bf16[48,40,512]{2,1,0:T(8,128)(2,1)}), bf16[48,40,512]{2,1,0:T(8,128)(2,1)S(1)}, u32[]{:S(2)}, u32[]{:S(2)}) async-start(bf16[48,40,512]{2,1,0:T(8,128)(2,1)} %ffn.1), calls=%async_computation.1 | async-start | bytes 3932160 | tf_op jit(solution)/shard_map/all_to_all | solution.py:228
  117.0 0.0 copy-done.4
  117.0 0.1 copy.17.ids_ref
  117.1 0.0 copy-done.3
  117.2 0.1 copy.16
  117.3 0.0 copy-done.5
  117.3 0.1 broadcast_multiply_fusion.weight_ref
  117.4 50.8 %all-to-all-done.1.back_ref = bf16[48,40,512]{2,1,0:T(8,128)(2,1)S(1)} async-done(((bf16[48,40,512]{2,1,0:T(8,128)(2,1)}), bf16[48,40,512]{2,1,0:T(8,128)(2,1)S(1)}, u32[]{:S(2)}, u32[]{:S(2)}) %all-to-all-start.1) | async-done | bytes 1966112 | tf_op jit(solution)/shard_map/all_to_all | solution.py:228
  168.2 0.0 copy-done
  168.2 0.0 copy-done.1
  168.2 0.0 copy-done.2
  168.2 3.1 %mix.1 = bf16[160,2048]{1,0:T(8,128)(2,1)} custom-call(bf16[48,40,512]{2,1,0:T(8,128)(2,1)S(1)} %all-to-all-done.1.back_ref, bf16[160,2048]{1,0:T(8,128)(2,1)S(1)} %copy-done, s32[160,2]{1,0:T(8,128)S(1)} %copy.17.ids_ref, f32[160,2]{1,0:T(8,128)S(1)} %broadcast_multiply_fusion.weight_ref, f32[1,2048]{1,0:T(1,128)S(1)} %bitcast.8, f32[1,2048]{1,0:T(1,128)S(1)} %bitcast.9), custom_call_target="tpu_custom_call" | custom-call | tf_op jit(solution)/shard_map/mix/pallas_call | solution.py:231
  (3 shorter events, 0.0 us)
Async XLA Ops:
  6.5 97.9 %all-gather.2.cloned.1.call-start = ((), (), s32[]{:S(2)}) async-start(), calls=%async_computation.2 | async-start | bytes 6684672 | tf_op jit(solution)/shard_map/all_gather | solution.py:197
  111.8 5.2 %copy-start.4 = (s32[160,2]{0,1:T(2,128)S(1)}, s32[160,2]{0,1:T(2,128)}, u32[]{:S(2)}) copy-start(s32[160,2]{0,1:T(2,128)} %param.10) | copy-start | bytes 3844
  111.9 5.3 %copy-start.3 = (f32[160,2]{0,1:T(2,128)S(1)}, f32[160,2]{0,1:T(2,128)}, u32[]{:S(2)}) copy-start(f32[160,2]{0,1:T(2,128)} %param.12) | copy-start | bytes 3844
  111.9 5.4 %copy-start.5 = (f32[160]{0:T(256)S(1)}, f32[160]{0:T(256)}, u32[]{:S(2)}) copy-start(f32[160]{0:T(256)} %param.11) | copy-start | bytes 1924
  111.9 56.3 %copy-start = (bf16[160,2048]{1,0:T(8,128)(2,1)S(1)}, bf16[160,2048]{1,0:T(8,128)(2,1)}, u32[]{:S(2)}) copy-start(bf16[160,2048]{1,0:T(8,128)(2,1)} %tok_ref.3) | copy-start | bytes 1966084
  111.9 56.3 %copy-start.1 = (f32[2048]{0:T(1024)S(1)}, f32[2048]{0:T(1024)}, u32[]{:S(2)}) copy-start(f32[2048]{0:T(1024)} %param.16) | copy-start | bytes 24580
  111.9 56.3 %copy-start.2 = (f32[2048]{0:T(1024)S(1)}, f32[2048]{0:T(1024)}, u32[]{:S(2)}) copy-start(f32[2048]{0:T(1024)} %param.17) | copy-start | bytes 24580
  111.9 56.3 %all-to-all-start.1 = ((bf16[48,40,512]{2,1,0:T(8,128)(2,1)}), bf16[48,40,512]{2,1,0:T(8,128)(2,1)S(1)}, u32[]{:S(2)}, u32[]{:S(2)}) async-start(bf16[48,40,512]{2,1,0:T(8,128)(2,1)} %ffn.1), calls=%async_computation.1 | async-start | bytes 3932160 | tf_op jit(solution)/shard_map/all_to_all | solution.py:228
Sparse Core Ops, SparseCore 0:
  9.7 59.2 all-gather.1
